TPU v7x, 512 devices: a whole 4x4x16 slice. The times are simulated.
512 devices in a mesh: fs: 128 (over z, x, core), tp: 4 (over y).
Axes of the slice: x: 4, y: 4, z: 16, core: 2. Of those that a mesh axis runs over, the one named last changes fastest.
Arguments:
- layer_input: bfloat16 [98304, 2048], P('fs'), may hold values from -6 to 6
- branch_cotangent: bfloat16 [98304, 1024], P('fs', 'tp'), may hold values from -0.014343262 to 0.014343262
- gate_cotangent: bfloat16 [98304, 1024], P('fs', 'tp'), may hold values from -0.014343262 to 0.014343262
- branch_factor: bfloat16 [2048, 128], P('fs'), may hold values from -0.5 to 0.5
- gate_factor: bfloat16 [2048, 128], P('fs'), may hold values from -0.5 to 0.5
- branch_weight: float32 [2048, 1024], P('fs', 'tp'), may hold values from -6 to 6
- gate_weight: float32 [2048, 1024], P('fs', 'tp'), may hold values from -6 to 6
- branch_first: float32 [128, 1024], P(None, 'tp'), may hold values from -6 to 6
- gate_first: float32 [128, 1024], P(None, 'tp'), may hold values from -6 to 6
- branch_second: float32 [128, 1024], P(None, 'tp'), may hold values from 0.0625 to 900
- gate_second: float32 [128, 1024], P(None, 'tp'), may hold values from 0.0625 to 900
Outputs:
- branch_step: float32 [2048, 1024], P('fs', 'tp')
- gate_step: float32 [2048, 1024], P('fs', 'tp')
- branch_new: float32 [2048, 1024], P('fs', 'tp')
- gate_new: float32 [2048, 1024], P('fs', 'tp')
- branch_copy: bfloat16 [2048, 1024], P(None, 'tp')
- gate_copy: bfloat16 [2048, 1024], P(None, 'tp')
- branch_first_new: float32 [128, 1024], P(None, 'tp')
- gate_first_new: float32 [128, 1024], P(None, 'tp')
- branch_second_new: float32 [128, 1024], P(None, 'tp')
- gate_second_new: float32 [128, 1024], P(None, 'tp')
All inputs are finite; a program needn't handle non-finite values.
Results may differ from a plain program's by a relative error of at most 0.00055.
Values may be sent and summed in bfloat16 or wider, within the bound.
No kernel may reach another device: no remote copies, remote signals or barrier semaphores. Data moves between devices by JAX's collectives and lax.ppermute only.
A program may use at most 64 MiB of HBM per device.

v0:
```python
import functools

import jax
import jax.numpy as jnp
from jax import lax
from jax.experimental import pallas as pl
from jax.experimental.pallas import tpu as pltpu
from jax.sharding import Mesh
from jax.sharding import PartitionSpec as P


FS = ("zh", "zl", "x", "c")
FAR = ("zh",)
NEAR = ("zl", "x")
NEAR_CORES = ("zl", "x", "c")

first_decay = 0.8
second_decay = 0.9
learn_rate = 0.5


def size_of(axes):
    peers = 1
    for a in axes:
        peers *= lax.axis_size(a)
    return peers


def exchanged(blocks, axes):
    return lax.all_to_all(blocks, axes, split_axis=0, concat_axis=0, tiled=True)


def from_everyone(x, axes):
    return exchanged(jnp.broadcast_to(x, (size_of(axes), *x.shape)), axes)


def swapped(x):
    return lax.ppermute(x, "c", [(0, 1), (1, 0)])


def two_parts(x):
    high = lax.reduce_precision(x, 8, 7)
    return high.astype(jnp.bfloat16), (x - high).astype(jnp.bfloat16)


def projected_locally(rows, cotangent):
    high, low = two_parts(rows)
    rank = rows.shape[1]
    both = lax.dot_general(
        jnp.concatenate([high, low], axis=1),
        cotangent,
        (((0,), (0,)), ((), ())),
        preferred_element_type=jnp.float32,
    )
    return both[:rank] + both[rank:]


def moved_and_spread(projected, first, second):
    moved = first_decay * first + (1.0 - first_decay) * projected
    spread = second_decay * second + (1.0 - second_decay) * projected * projected
    return moved, spread


def direction_kernel(
    projected, branch_first, gate_first, branch_second, gate_second, parts, squares
):
    rank, width = branch_first.shape
    total = jnp.zeros((8, 128), jnp.float32)
    both = ((branch_first, branch_second), (gate_first, gate_second))
    for p, (first, second) in enumerate(both):
        moved, spread = moved_and_spread(projected[p], first[...], second[...])
        direction = moved / jnp.sqrt(spread)
        high = direction.astype(jnp.bfloat16)
        rest = direction - high.astype(jnp.float32)
        middle = rest.astype(jnp.bfloat16)
        low = (rest - middle.astype(jnp.float32)).astype(jnp.bfloat16)
        parts[p, :, :width] = high
        parts[p, :, width : 2 * width] = middle
        parts[p, :, 2 * width :] = low
        squared = direction * direction
        for column in range(0, width, 128):
            total += jnp.sum(
                squared[:, column : column + 128].reshape(rank // 8, 8, 128), axis=0
            )
    squares[...] = total


def scale_of(entries, squares):
    total = jnp.sum(jnp.sum(squares, axis=0), keepdims=True)
    return -learn_rate / jnp.sqrt(total / entries + 1e-06)


def times_parts(factor, parts):
    width = parts.shape[1] // 3
    out = jnp.dot(factor, parts, preferred_element_type=jnp.float32)
    return out[:, :width] + (out[:, width : 2 * width] + out[:, 2 * width :])


def rows_kernel(entries, squares, parts, factors, arrived, rows_new):
    far, block, _ = factors.shape
    rank = parts.shape[1]
    width = arrived.shape[2]
    minus_scale = scale_of(entries, squares[...])
    for p in range(2):
        factor = factors[:, :, p * rank : (p + 1) * rank].reshape(far * block, rank)
        step = (minus_scale * times_parts(factor, parts[p])).reshape(far, block, width)
        weights = arrived[:, (p + 1) * block : (p + 2) * block, :]
        rows_new[:, :, p * width : (p + 1) * width] = (weights + step).astype(jnp.bfloat16)


def results_kernel(
    entries,
    projected,
    branch_first,
    gate_first,
    branch_second,
    gate_second,
    squares,
    parts,
    branch_factor,
    gate_factor,
    branch_weight,
    gate_weight,
    branch_step,
    gate_step,
    branch_new,
    gate_new,
    branch_first_new,
    gate_first_new,
    branch_second_new,
    gate_second_new,
):
    minus_scale = scale_of(entries, squares[...])
    both = (
        (branch_first, branch_second, branch_first_new, branch_second_new),
        (gate_first, gate_second, gate_first_new, gate_second_new),
    )
    for p, (first, second, first_new, second_new) in enumerate(both):
        moved, spread = moved_and_spread(projected[p], first[...], second[...])
        first_new[...] = moved
        second_new[...] = spread
    rows = (
        (branch_factor, branch_weight, branch_step, branch_new),
        (gate_factor, gate_weight, gate_step, gate_new),
    )
    for p, (factor, weight, step_out, new_out) in enumerate(rows):
        step = minus_scale * times_parts(factor[...], parts[p])
        step_out[...] = step
        new_out[...] = weight[...] + step


def outgoing_kernel(pieces, branch_weight, gate_weight, outgoing_block):
    height = pieces.shape[1]
    block = branch_weight.shape[0]
    outgoing_block[:height] = jnp.sum(pieces[...], axis=0)
    outgoing_block[height : height + block] = branch_weight[...]
    outgoing_block[height + block :] = gate_weight[...]


def factors_kernel(mine, other, factors):
    near_z, near_x, far, block, _ = mine.shape
    core = lax.axis_index("c")
    for f in range(far):
        for z in range(near_z):
            for x in range(near_x):
                row = ((f * near_z + z) * near_x + x) * 2 * block
                for source, place in ((mine, core), (other, 1 - core)):
                    rows = pl.ds(pl.multiple_of(row + place * block, block), block)
                    factors[rows, :] = source[z, x, f]


def placed(blocks, place, copies, done):
    near_z, near_x = blocks.shape[:2]
    width = copies[0].shape[-1]
    started = []
    for p, copy in enumerate(copies):
        for z in range(near_z):
            for x in range(near_x):
                started.append(
                    pltpu.make_async_copy(
                        blocks.at[z, x, :, :, pl.ds(p * width, width)],
                        copy.at[:, z, x, place],
                        done.at[len(started)],
                    )
                )
    for one in started:
        one.start()
    for one in started:
        one.wait()


def mine_kernel(mine, branch_copy, gate_copy, done):
    placed(mine, lax.axis_index("c"), (branch_copy, gate_copy), done)


def other_kernel(other, branch_in, gate_in, branch_copy, gate_copy, done):
    del branch_in, gate_in
    placed(other, 1 - lax.axis_index("c"), (branch_copy, gate_copy), done)


def whole():
    return pl.BlockSpec(memory_space=pltpu.VMEM)


def anywhere():
    return pl.BlockSpec(memory_space=pl.ANY)


def grant(mib):
    return pltpu.CompilerParams(vmem_limit_bytes=mib << 20)


def outgoing(pieces, branch_weight, gate_weight):
    height = pieces.shape[1] + 2 * branch_weight.shape[0]
    return pl.pallas_call(
        outgoing_kernel,
        out_shape=jax.ShapeDtypeStruct((height, pieces.shape[2]), jnp.float32),
        in_specs=[whole()] * 3,
        out_specs=whole(),
        compiler_params=grant(4),
        name="outgoing",
    )(pieces, branch_weight, gate_weight)


def whole_factors(mine, other):
    near_z, near_x, far, block, columns = mine.shape
    return pl.pallas_call(
        factors_kernel,
        out_shape=jax.ShapeDtypeStruct((2 * near_z * near_x * far * block, columns), mine.dtype),
        in_specs=[whole()] * 2,
        out_specs=whole(),
        compiler_params=grant(4),
        name="whole_factors",
    )(mine, other)


def copies_of(mine):
    near_z, near_x, far, block, columns = mine.shape
    copy = jax.ShapeDtypeStruct((far, near_z, near_x, 2, block, columns // 2), mine.dtype)
    return [copy, copy], [pltpu.SemaphoreType.DMA((2 * near_z * near_x,))]


def place_mine(mine):
    shapes, scratch = copies_of(mine)
    return pl.pallas_call(
        mine_kernel,
        out_shape=shapes,
        in_specs=[whole()],
        out_specs=[anywhere()] * 2,
        scratch_shapes=scratch,
        compiler_params=grant(4),
        cost_estimate=pl.CostEstimate(flops=1 << 20, bytes_accessed=1 << 21, transcendentals=0),
        name="place_mine",
    )(mine)


def place_other(other, branch_copy, gate_copy):
    shapes, scratch = copies_of(other)
    return pl.pallas_call(
        other_kernel,
        out_shape=shapes,
        in_specs=[whole(), anywhere(), anywhere()],
        out_specs=[anywhere()] * 2,
        scratch_shapes=scratch,
        input_output_aliases={1: 0, 2: 1},
        compiler_params=grant(4),
        name="place_other",
    )(other, branch_copy, gate_copy)


def directions(projected, branch_first, gate_first, branch_second, gate_second):
    rank, width = branch_first.shape
    return pl.pallas_call(
        direction_kernel,
        out_shape=[
            jax.ShapeDtypeStruct((2, rank, 3 * width), jnp.bfloat16),
            jax.ShapeDtypeStruct((8, 128), jnp.float32),
        ],
        in_specs=[whole()] * 5,
        out_specs=[whole()] * 2,
        compiler_params=grant(6),
        name="directions",
    )(projected, branch_first, gate_first, branch_second, gate_second)


def new_rows(entries, squares, parts, factors, arrived):
    far, block, _ = factors.shape
    return pl.pallas_call(
        functools.partial(rows_kernel, entries),
        out_shape=jax.ShapeDtypeStruct((far, block, 2 * arrived.shape[2]), jnp.bfloat16),
        in_specs=[whole()] * 4,
        out_specs=whole(),
        compiler_params=grant(6),
        name="new_rows",
    )(squares, parts, factors, arrived)


def results(entries, projected, moments, squares, parts, factors, weights):
    rank, width = moments[0].shape
    block = weights[0].shape[0]
    row = jax.ShapeDtypeStruct((block, width), jnp.float32)
    moment = jax.ShapeDtypeStruct((rank, width), jnp.float32)
    return pl.pallas_call(
        functools.partial(results_kernel, entries),
        out_shape=[row] * 4 + [moment] * 4,
        in_specs=[whole()] * 11,
        out_specs=[whole()] * 8,
        compiler_params=grant(6),
        cost_estimate=pl.CostEstimate(flops=1 << 22, bytes_accessed=1 << 21, transcendentals=0),
        name="results",
    )(projected, *moments, squares, parts, *factors, *weights)


def body(
    layer_input,
    branch_cotangent,
    gate_cotangent,
    branch_factor,
    gate_factor,
    branch_weight,
    gate_weight,
    branch_first,
    gate_first,
    branch_second,
    gate_second,
):
    rank, width = branch_first.shape
    near = (lax.axis_size("zl"), lax.axis_size("x"))

    far_factors = from_everyone(jnp.concatenate([branch_factor, gate_factor], axis=1), FAR)
    near_factors = from_everyone(far_factors, NEAR).reshape(*near, *far_factors.shape)
    factors = whole_factors(near_factors, swapped(near_factors))

    rows = jnp.dot(layer_input, factors, preferred_element_type=jnp.float32)
    both = jnp.stack(
        [
            projected_locally(rows[:, :rank], branch_cotangent),
            projected_locally(rows[:, rank:], gate_cotangent),
        ]
    )
    pieces = both.reshape(size_of(NEAR_CORES), -1, width)
    height = pieces.shape[1]
    outgoing_block = outgoing(exchanged(pieces, NEAR_CORES), branch_weight, gate_weight)
    arrived = lax.all_gather(outgoing_block, "zh")
    total = arrived[:, :height].sum(axis=0)
    projected = from_everyone(total, NEAR_CORES).reshape(both.shape)

    entries = 2 * rank * width * lax.axis_size("tp")
    moments = (branch_first, gate_first, branch_second, gate_second)
    parts, squares = directions(projected, *moments)
    squares = from_everyone(squares, ("tp",))
    rows_new = new_rows(entries, squares, parts, far_factors, arrived)

    mine = from_everyone(rows_new, NEAR).reshape(*near, *rows_new.shape)
    other = swapped(mine)
    copies = place_mine(mine)
    (
        branch_step,
        gate_step,
        branch_new,
        gate_new,
        branch_first_new,
        gate_first_new,
        branch_second_new,
        gate_second_new,
    ) = results(
        entries,
        projected,
        moments,
        squares,
        parts,
        (branch_factor, gate_factor),
        (branch_weight, gate_weight),
    )
    branch_copy, gate_copy = [c.reshape(-1, width) for c in place_other(other, *copies)]
    return (
        branch_step,
        gate_step,
        branch_new,
        gate_new,
        branch_copy,
        gate_copy,
        branch_first_new,
        gate_first_new,
        branch_second_new,
        gate_second_new,
    )


def solution(mesh):
    finer = Mesh(
        mesh.devices.reshape(8, 2, 4, 2, mesh.shape["tp"]), ("zh", "zl", "x", "c", "tp")
    )
    sharded = P(FS, None)
    split = P(FS, "tp")
    kept = P(None, "tp")
    in_specs = (sharded, split, split, sharded, sharded, split, split, kept, kept, kept, kept)
    out_specs = (split, split, split, split, kept, kept, kept, kept, kept, kept)
    return jax.shard_map(body, mesh=finer, in_specs=in_specs, out_specs=out_specs, check_vma=False)
```

profile of v0, /device:TPU:1, one launch (start us, length us, event | category | flops | bytes accessed | tf_op | source)
XLA Modules:
  0.0 133.6 jit_solution(4530542209644700901)
XLA Ops:
  0.6 0.0 copy-start
  0.7 0.9 pad_maximum_fusion.1
  1.5 27.8 %all_to_all.30.factors = bf16[8,16,256]{2,1,0:T(8,128)(2,1)S(1)} all-to-all(bf16[8,16,256]{2,1,0:T(8,128)(2,1)S(1)} %broadcast_in_dim.15), channel_id=1, replica_groups=mesh['zh'=8,'zl'=2,'x'=4,'c'=2,'tp'=4] {'zh'}, dimensions={0} | all-to-all | bytes 131072 | tf_op jit(solution)/shard_map/all_to_all | solution.py:30
  29.3 11.4 %all_to_all.31 = bf16[8,8,16,256]{3,2,1,0:T(8,128)(2,1)S(1)} all-to-all(bf16[8,8,16,256]{3,2,1,0:T(8,128)(2,1)S(1)} %broadcast_in_dim.16), channel_id=1, replica_groups=mesh['zh'=8,'zl'=2,'x'=4,'c'=2,'tp'=4] {'zl','x'}, dimensions={0} | all-to-all | bytes 1048576 | tf_op jit(solution)/shard_map/all_to_all | solution.py:30
  40.7 6.0 %collective-permute-start = (bf16[2,4,8,16,256]{4,3,2,1,0:T(8,128)(2,1)S(1)}, bf16[2,4,8,16,256]{4,3,2,1,0:T(8,128)(2,1)S(1)}, u32[]{:S(2)}, u32[]{:S(2)}) collective-permute-start(bf16[2,4,8,16,256]{4,3,2,1,0:T(8,128)(2,1)S(1)} %bitcast.23), channel_id=1, source_target_pairs={{0,4},{4,0},{1,5},{5,1},{2,6},{6,2},{3,7},{7,3},{8,12},{12,8},{9,1... | collective-permute-start | bytes 1572872 | tf_op jit(solution)/shard_map/ppermute | solution.py:38
  46.8 1.5 %collective-permute-done.other = bf16[2,4,8,16,256]{4,3,2,1,0:T(8,128)(2,1)S(1)} collective-permute-done((bf16[2,4,8,16,256]{4,3,2,1,0:T(8,128)(2,1)S(1)}, bf16[2,4,8,16,256]{4,3,2,1,0:T(8,128)(2,1)S(1)}, u32[]{:S(2)}, u32[]{:S(2)}) %collective-permute-start) | collective-permute-done | bytes 524320 | tf_op jit(solution)/shard_map/ppermute | solution.py:38
  48.3 0.1 whole_factors.1
  48.5 1.1 convolution_bitcast_fusion
  49.6 0.1 reduce-precision_convert_fusion.1
  49.7 0.3 fusion.2
  50.0 0.3 fusion.6
  50.4 10.2 %all_to_all.32.pieces = f32[16,16,256]{2,1,0:T(8,128)S(1)} all-to-all(f32[16,16,256]{2,1,0:T(8,128)S(1)} %bitcast.27), channel_id=1, replica_groups=mesh['zh'=8,'zl'=2,'x'=4,'c'=2,'tp'=4] {'zl','x','c'}, dimensions={0} | all-to-all | bytes 524288 | tf_op jit(solution)/shard_map/all_to_all | solution.py:30
  60.6 22.8 %all-gather = f32[384,256]{1,0:T(8,128)S(1)} all-gather(f32[48,256]{1,0:T(8,128)S(1)} %outgoing.1), channel_id=2, replica_groups=mesh['zh'=8,'zl'=2,'x'=4,'c'=2,'tp'=4] {'zh'}, dimensions={0}, use_global_device_ids=true | all-gather | bytes 442368 | tf_op jit(solution)/shard_map/all_gather | solution.py:344
  83.5 16.9 %all_to_all.33 = f32[16,16,256]{2,1,0:T(8,128)S(1)} all-to-all(f32[16,16,256]{2,1,0:T(8,128)S(1)} %broadcast_in_dim.17), channel_id=1, replica_groups=mesh['zh'=8,'zl'=2,'x'=4,'c'=2,'tp'=4] {'zl','x','c'}, dimensions={0} | all-to-all | bytes 524288 | tf_op jit(solution)/shard_map/all_to_all | solution.py:30
  100.4 0.2 directions.1
  100.6 8.1 %all_to_all.34.squares = f32[4,8,128]{2,1,0:T(8,128)S(1)} all-to-all(f32[4,8,128]{2,1,0:T(8,128)S(1)} %broadcast_in_dim.18), channel_id=1, replica_groups=mesh['zh'=8,'zl'=2,'x'=4,'c'=2,'tp'=4] {'tp'}, dimensions={0} | all-to-all | bytes 32768 | tf_op jit(solution)/shard_map/all_to_all | solution.py:30
  108.8 0.3 new_rows.1
  109.1 0.1 broadcast_in_dim.19
  109.2 15.4 %all_to_all.35 = bf16[8,8,16,512]{3,2,1,0:T(8,128)(2,1)S(1)} all-to-all(bf16[8,8,16,512]{3,2,1,0:T(8,128)(2,1)S(1)} %broadcast_in_dim.19), channel_id=1, replica_groups=mesh['zh'=8,'zl'=2,'x'=4,'c'=2,'tp'=4] {'zl','x'}, dimensions={0} | all-to-all | bytes 2097152 | tf_op jit(solution)/shard_map/all_to_all | solution.py:30
  124.6 5.7 %collective-permute-start.1 = (bf16[2,4,8,16,512]{4,3,2,1,0:T(8,128)(2,1)S(1)}, bf16[2,4,8,16,512]{4,3,2,1,0:T(8,128)(2,1)S(1)}, u32[]{:S(2)}, u32[]{:S(2)}) collective-permute-start(bf16[2,4,8,16,512]{4,3,2,1,0:T(8,128)(2,1)S(1)} %bitcast.17), channel_id=1, source_target_pairs={{0,4},{4,0},{1,5},{5,1},{2,6},{6,2},{3,7},{7,3},{8,12},{12,8},{9,1... | collective-permute-start | bytes 3145736 | tf_op jit(solution)/shard_map/ppermute | solution.py:38
  130.3 0.9 results.1
  131.2 1.1 place_mine.1
  132.3 0.2 collective-permute-done.1.other
  132.5 1.1 place_other.1
  (29 shorter events, 0.2 us)
Async XLA Ops:
  0.6 47.8 %copy-start = (bf16[768,2048]{1,0:T(8,128)(2,1)S(1)}, bf16[768,2048]{1,0:T(8,128)(2,1)}, u32[]{:S(2)}) copy-start(bf16[768,2048]{1,0:T(8,128)(2,1)} %param.11) | copy-start | bytes 9437188
  40.7 7.6 %collective-permute-start = (bf16[2,4,8,16,256]{4,3,2,1,0:T(8,128)(2,1)S(1)}, bf16[2,4,8,16,256]{4,3,2,1,0:T(8,128)(2,1)S(1)}, u32[]{:S(2)}, u32[]{:S(2)}) collective-permute-start(bf16[2,4,8,16,256]{4,3,2,1,0:T(8,128)(2,1)S(1)} %bitcast.23), channel_id=1, source_target_pairs={{0,4},{4,0},{1,5},{5,1},{2,6},{6,2},{3,7},{7,3},{8,12},{12,8},{9,1... | collective-permute-start | bytes 1572872 | tf_op jit(solution)/shard_map/ppermute | solution.py:38
  48.4 1.3 copy-start.9
  48.4 1.6 %copy-start.10 = (bf16[768,256]{1,0:T(8,128)(2,1)S(1)}, bf16[768,256]{1,0:T(8,128)(2,1)}, u32[]{:S(2)}) copy-start(bf16[768,256]{1,0:T(8,128)(2,1)} %param.13) | copy-start | bytes 1179652
  49.6 11.0 %copy-start.5 = (f32[16,256]{1,0:T(8,128)S(1)}, f32[16,256]{1,0:T(8,128)}, u32[]{:S(2)}) copy-start(f32[16,256]{1,0:T(8,128)} %branch_weight.3) | copy-start | bytes 49156
  49.6 11.0 %copy-start.6 = (f32[16,256]{1,0:T(8,128)S(1)}, f32[16,256]{1,0:T(8,128)}, u32[]{:S(2)}) copy-start(f32[16,256]{1,0:T(8,128)} %gate_weight.3) | copy-start | bytes 49156
  49.7 50.7 %copy-start.1 = (f32[128,256]{1,0:T(8,128)S(1)}, f32[128,256]{1,0:T(8,128)}, u32[]{:S(2)}) copy-start(f32[128,256]{1,0:T(8,128)} %branch_first.3) | copy-start | bytes 393220
  49.7 50.7 %copy-start.2 = (f32[128,256]{1,0:T(8,128)S(1)}, f32[128,256]{1,0:T(8,128)}, u32[]{:S(2)}) copy-start(f32[128,256]{1,0:T(8,128)} %gate_first.3) | copy-start | bytes 393220
  49.7 50.7 %copy-start.3 = (f32[128,256]{1,0:T(8,128)S(1)}, f32[128,256]{1,0:T(8,128)}, u32[]{:S(2)}) copy-start(f32[128,256]{1,0:T(8,128)} %branch_second.3) | copy-start | bytes 393220
  49.7 50.7 %copy-start.4 = (f32[128,256]{1,0:T(8,128)S(1)}, f32[128,256]{1,0:T(8,128)}, u32[]{:S(2)}) copy-start(f32[128,256]{1,0:T(8,128)} %gate_second.3) | copy-start | bytes 393220
  83.4 46.9 %copy-start.7 = (bf16[16,128]{1,0:T(8,128)(2,1)S(1)}, bf16[16,128]{1,0:T(8,128)(2,1)}, u32[]{:S(2)}) copy-start(bf16[16,128]{1,0:T(8,128)(2,1)} %gate_factor.1) | copy-start | bytes 12292
  83.4 46.9 %copy-start.8 = (bf16[16,128]{1,0:T(8,128)(2,1)S(1)}, bf16[16,128]{1,0:T(8,128)(2,1)}, u32[]{:S(2)}) copy-start(bf16[16,128]{1,0:T(8,128)(2,1)} %branch_factor.1) | copy-start | bytes 12292
  124.6 8.0 %collective-permute-start.1 = (bf16[2,4,8,16,512]{4,3,2,1,0:T(8,128)(2,1)S(1)}, bf16[2,4,8,16,512]{4,3,2,1,0:T(8,128)(2,1)S(1)}, u32[]{:S(2)}, u32[]{:S(2)}) collective-permute-start(bf16[2,4,8,16,512]{4,3,2,1,0:T(8,128)(2,1)S(1)} %bitcast.17), channel_id=1, source_target_pairs={{0,4},{4,0},{1,5},{5,1},{2,6},{6,2},{3,7},{7,3},{8,12},{12,8},{9,1... | collective-permute-start | bytes 3145736 | tf_op jit(solution)/shard_map/ppermute | solution.py:38
where the time goes:
time: 134 us
  blocking collectives  113 us (84%)
  starting transfers between devices  11.7 us (9%)
  Pallas kernels  3.75 us (3%)
  waiting for transfers between devices  1.72 us (1%)
  matrix products  1.62 us (1%)
    all_to_all x6, blocking collectives, exchanged(): return lax.all_to_all(blocks, axes, split_axis=0, concat_axis=0, tiled=True)  89.8 us
    all_gather x1, blocking collectives, body(): arrived = lax.all_gather(outgoing_block, 'zh')  22.8 us
    ppermute x2, starting transfers between devices, swapped(): return lax.ppermute(x, 'c', [(0, 1), (1, 0)])  11.7 us
  transfers between devices with their start and end apart: 2, of which 2 were waited for; matrix products, arithmetic and copies ran while one was open for 0% of the time, Pallas kernels for 2%

commit v1 on v0

--- a/solution.py
+++ b/solution.py
@@ -11,6 +11,7 @@
 
 FS = ("zh", "zl", "x", "c")
 FAR = ("zh",)
+Z = ("zh", "zl")
 NEAR = ("zl", "x")
 NEAR_CORES = ("zl", "x", "c")
 
@@ -61,6 +62,11 @@
     return moved, spread
 
 
+def part_of(projected, p):
+    groups, _, height, width = projected.shape
+    return projected[:, p].reshape(groups * height, width)
+
+
 def direction_kernel(
     projected, branch_first, gate_first, branch_second, gate_second, parts, squares
 ):
@@ -68,7 +74,7 @@
     total = jnp.zeros((8, 128), jnp.float32)
     both = ((branch_first, branch_second), (gate_first, gate_second))
     for p, (first, second) in enumerate(both):
-        moved, spread = moved_and_spread(projected[p], first[...], second[...])
+        moved, spread = moved_and_spread(part_of(projected, p), first[...], second[...])
         direction = moved / jnp.sqrt(spread)
         high = direction.astype(jnp.bfloat16)
         rest = direction - high.astype(jnp.float32)
@@ -97,15 +103,17 @@
 
 
 def rows_kernel(entries, squares, parts, factors, arrived, rows_new):
-    far, block, _ = factors.shape
+    near_z, _, far, block, _ = factors.shape
     rank = parts.shape[1]
-    width = arrived.shape[2]
+    width = arrived.shape[3]
+    x = lax.axis_index("x")
     minus_scale = scale_of(entries, squares[...])
-    for p in range(2):
-        factor = factors[:, :, p * rank : (p + 1) * rank].reshape(far * block, rank)
-        step = (minus_scale * times_parts(factor, parts[p])).reshape(far, block, width)
-        weights = arrived[:, (p + 1) * block : (p + 2) * block, :]
-        rows_new[:, :, p * width : (p + 1) * width] = (weights + step).astype(jnp.bfloat16)
+    for z in range(near_z):
+        for p in range(2):
+            factor = factors[z, x, :, :, p * rank : (p + 1) * rank].reshape(far * block, rank)
+            step = (minus_scale * times_parts(factor, parts[p])).reshape(far, block, width)
+            weights = arrived[:, z, (p + 1) * block : (p + 2) * block, :]
+            rows_new[z, :, :, p * width : (p + 1) * width] = (weights + step).astype(jnp.bfloat16)
 
 
 def results_kernel(
@@ -136,7 +144,7 @@
         (gate_first, gate_second, gate_first_new, gate_second_new),
     )
     for p, (first, second, first_new, second_new) in enumerate(both):
-        moved, spread = moved_and_spread(projected[p], first[...], second[...])
+        moved, spread = moved_and_spread(part_of(projected, p), first[...], second[...])
         first_new[...] = moved
         second_new[...] = spread
     rows = (
@@ -170,7 +178,7 @@
 
 
 def placed(blocks, place, copies, done):
-    near_z, near_x = blocks.shape[:2]
+    near_x, near_z = blocks.shape[:2]
     width = copies[0].shape[-1]
     started = []
     for p, copy in enumerate(copies):
@@ -178,7 +186,7 @@
             for x in range(near_x):
                 started.append(
                     pltpu.make_async_copy(
-                        blocks.at[z, x, :, :, pl.ds(p * width, width)],
+                        blocks.at[x, z, :, :, pl.ds(p * width, width)],
                         copy.at[:, z, x, place],
                         done.at[len(started)],
                     )
@@ -235,7 +243,7 @@
 
 
 def copies_of(mine):
-    near_z, near_x, far, block, columns = mine.shape
+    near_x, near_z, far, block, columns = mine.shape
     copy = jax.ShapeDtypeStruct((far, near_z, near_x, 2, block, columns // 2), mine.dtype)
     return [copy, copy], [pltpu.SemaphoreType.DMA((2 * near_z * near_x,))]
 
@@ -284,13 +292,14 @@
 
 
 def new_rows(entries, squares, parts, factors, arrived):
-    far, block, _ = factors.shape
+    near_z, _, far, block, _ = factors.shape
+    columns = 2 * arrived.shape[3]
     return pl.pallas_call(
         functools.partial(rows_kernel, entries),
-        out_shape=jax.ShapeDtypeStruct((far, block, 2 * arrived.shape[2]), jnp.bfloat16),
+        out_shape=jax.ShapeDtypeStruct((near_z, far, block, columns), jnp.bfloat16),
         in_specs=[whole()] * 4,
         out_specs=whole(),
-        compiler_params=grant(6),
+        compiler_params=grant(8),
         name="new_rows",
     )(squares, parts, factors, arrived)
 
@@ -341,17 +350,17 @@
     pieces = both.reshape(size_of(NEAR_CORES), -1, width)
     height = pieces.shape[1]
     outgoing_block = outgoing(exchanged(pieces, NEAR_CORES), branch_weight, gate_weight)
-    arrived = lax.all_gather(outgoing_block, "zh")
-    total = arrived[:, :height].sum(axis=0)
-    projected = from_everyone(total, NEAR_CORES).reshape(both.shape)
+    arrived = lax.all_gather(outgoing_block, Z).reshape(-1, near[0], *outgoing_block.shape)
+    total = arrived[:, :, :height].sum(axis=0)
+    projected = from_everyone(total, ("x", "c"))
 
     entries = 2 * rank * width * lax.axis_size("tp")
     moments = (branch_first, gate_first, branch_second, gate_second)
     parts, squares = directions(projected, *moments)
     squares = from_everyone(squares, ("tp",))
-    rows_new = new_rows(entries, squares, parts, far_factors, arrived)
-
-    mine = from_everyone(rows_new, NEAR).reshape(*near, *rows_new.shape)
+    rows_new = new_rows(entries, squares, parts, near_factors, arrived)
+
+    mine = from_everyone(rows_new, ("x",))
     other = swapped(mine)
     copies = place_mine(mine)
     (

time: 134 us -> 135 us (level)
    all_gather x1, blocking collectives: 22.8 us -> 24.7 us  [body(): lax.all_gather(outgoing_block, Z)]
where the time goes in v1:
time: 135 us; the launch traced here: 134 us
  blocking collectives  114 us (84%)
  starting transfers between devices  11.3 us (8%)
  Pallas kernels  3.85 us (3%)
  waiting for transfers between devices  1.72 us (1%)
  matrix products  1.62 us (1%)
    all_to_all x6, blocking collectives, exchanged(): return lax.all_to_all(blocks, axes, split_axis=0, concat_axis=0, tiled=True)  88.8 us
    all_gather x1, blocking collectives, body(): lax.all_gather(outgoing_block, Z)  24.7 us
    ppermute x2, starting transfers between devices, swapped(): return lax.ppermute(x, 'c', [(0, 1), (1, 0)])  11.3 us
  transfers between devices with their start and end apart: 2, of which 2 were waited for; matrix products, arithmetic and copies ran while one was open for 0% of the time, Pallas kernels for 2%

profile of v1, /device:TPU:1, one launch (start us, length us, event | category | flops | bytes accessed | tf_op | source)
XLA Modules:
  0.0 134.2 jit_solution(3137499082923242609)
XLA Ops:
  0.6 0.0 copy-start
  0.7 0.9 pad_maximum_fusion.1
  1.5 27.8 %all_to_all.30 = bf16[8,16,256]{2,1,0:T(8,128)(2,1)S(1)} all-to-all(bf16[8,16,256]{2,1,0:T(8,128)(2,1)S(1)} %broadcast_in_dim.15), channel_id=1, replica_groups=mesh['zh'=8,'zl'=2,'x'=4,'c'=2,'tp'=4] {'zh'}, dimensions={0} | all-to-all | bytes 131072 | tf_op jit(solution)/shard_map/all_to_all | solution.py:31
  29.3 11.4 %all_to_all.31 = bf16[8,8,16,256]{3,2,1,0:T(8,128)(2,1)S(1)} all-to-all(bf16[8,8,16,256]{3,2,1,0:T(8,128)(2,1)S(1)} %broadcast_in_dim.16), channel_id=1, replica_groups=mesh['zh'=8,'zl'=2,'x'=4,'c'=2,'tp'=4] {'zl','x'}, dimensions={0} | all-to-all | bytes 1048576 | tf_op jit(solution)/shard_map/all_to_all | solution.py:31
  40.7 6.0 %collective-permute-start = (bf16[2,4,8,16,256]{4,3,2,1,0:T(8,128)(2,1)S(1)}, bf16[2,4,8,16,256]{4,3,2,1,0:T(8,128)(2,1)S(1)}, u32[]{:S(2)}, u32[]{:S(2)}) collective-permute-start(bf16[2,4,8,16,256]{4,3,2,1,0:T(8,128)(2,1)S(1)} %bitcast.15), channel_id=1, source_target_pairs={{0,4},{4,0},{1,5},{5,1},{2,6},{6,2},{3,7},{7,3},{8,12},{12,8},{9,1... | collective-permute-start | bytes 1572872 | tf_op jit(solution)/shard_map/ppermute | solution.py:39
  46.8 1.5 %collective-permute-done.other = bf16[2,4,8,16,256]{4,3,2,1,0:T(8,128)(2,1)S(1)} collective-permute-done((bf16[2,4,8,16,256]{4,3,2,1,0:T(8,128)(2,1)S(1)}, bf16[2,4,8,16,256]{4,3,2,1,0:T(8,128)(2,1)S(1)}, u32[]{:S(2)}, u32[]{:S(2)}) %collective-permute-start) | collective-permute-done | bytes 524320 | tf_op jit(solution)/shard_map/ppermute | solution.py:39
  48.3 0.1 whole_factors.1
  48.5 1.1 convolution_bitcast_fusion
  49.6 0.1 reduce-precision_convert_fusion.1
  49.7 0.3 fusion.2
  50.0 0.3 fusion.6
  50.4 10.2 %all_to_all.32.pieces = f32[16,16,256]{2,1,0:T(8,128)S(1)} all-to-all(f32[16,16,256]{2,1,0:T(8,128)S(1)} %bitcast.22), channel_id=1, replica_groups=mesh['zh'=8,'zl'=2,'x'=4,'c'=2,'tp'=4] {'zl','x','c'}, dimensions={0} | all-to-all | bytes 524288 | tf_op jit(solution)/shard_map/all_to_all | solution.py:31
  60.6 24.7 %all-gather = f32[768,256]{1,0:T(8,128)S(1)} all-gather(f32[48,256]{1,0:T(8,128)S(1)} %outgoing.1), channel_id=2, replica_groups=mesh['zh'=8,'zl'=2,'x'=4,'c'=2,'tp'=4] {'zh','zl'}, dimensions={0}, use_global_device_ids=true | all-gather | bytes 835584 | tf_op jit(solution)/shard_map/all_gather | solution.py:353
  85.3 16.2 %all_to_all.33.projected = f32[8,2,16,256]{3,2,1,0:T(8,128)S(1)} all-to-all(f32[8,2,16,256]{3,2,1,0:T(8,128)S(1)} %broadcast_in_dim.17), channel_id=1, replica_groups=mesh['zh'=8,'zl'=2,'x'=4,'c'=2,'tp'=4] {'x','c'}, dimensions={0} | all-to-all | bytes 524288 | tf_op jit(solution)/shard_map/all_to_all | solution.py:31
  101.5 0.2 directions.1
  101.8 8.2 %all_to_all.34.squares = f32[4,8,128]{2,1,0:T(8,128)S(1)} all-to-all(f32[4,8,128]{2,1,0:T(8,128)S(1)} %broadcast_in_dim.18), channel_id=1, replica_groups=mesh['zh'=8,'zl'=2,'x'=4,'c'=2,'tp'=4] {'tp'}, dimensions={0} | all-to-all | bytes 32768 | tf_op jit(solution)/shard_map/all_to_all | solution.py:31
  110.0 0.4 new_rows.1
  110.3 0.1 broadcast_in_dim.19
  110.5 15.1 %all_to_all.35.mine = bf16[4,2,8,16,512]{4,3,2,1,0:T(8,128)(2,1)S(1)} all-to-all(bf16[4,2,8,16,512]{4,3,2,1,0:T(8,128)(2,1)S(1)} %broadcast_in_dim.19), channel_id=1, replica_groups=mesh['zh'=8,'zl'=2,'x'=4,'c'=2,'tp'=4] {'x'}, dimensions={0} | all-to-all | bytes 2097152 | tf_op jit(solution)/shard_map/all_to_all | solution.py:31
  125.6 5.2 %collective-permute-start.1 = (bf16[4,2,8,16,512]{4,3,2,1,0:T(8,128)(2,1)S(1)}, bf16[4,2,8,16,512]{4,3,2,1,0:T(8,128)(2,1)S(1)}, u32[]{:S(2)}, u32[]{:S(2)}) collective-permute-start(bf16[4,2,8,16,512]{4,3,2,1,0:T(8,128)(2,1)S(1)} %all_to_all.35.mine), channel_id=1, source_target_pairs={{0,4},{4,0},{1,5},{5,1},{2,6},{6,2},{3,7},{7,3},{8,12},{12,8},{9,1... | collective-permute-start | bytes 3145736 | tf_op jit(solution)/shard_map/ppermute | solution.py:39
  130.8 0.9 results.1
  131.8 1.1 place_mine.1
  132.9 0.2 collective-permute-done.1.other
  133.1 1.1 place_other.1
  (29 shorter events, 0.2 us)
Async XLA Ops:
  0.6 47.8 %copy-start = (bf16[768,2048]{1,0:T(8,128)(2,1)S(1)}, bf16[768,2048]{1,0:T(8,128)(2,1)}, u32[]{:S(2)}) copy-start(bf16[768,2048]{1,0:T(8,128)(2,1)} %param.11) | copy-start | bytes 9437188
  40.7 7.6 %collective-permute-start = (bf16[2,4,8,16,256]{4,3,2,1,0:T(8,128)(2,1)S(1)}, bf16[2,4,8,16,256]{4,3,2,1,0:T(8,128)(2,1)S(1)}, u32[]{:S(2)}, u32[]{:S(2)}) collective-permute-start(bf16[2,4,8,16,256]{4,3,2,1,0:T(8,128)(2,1)S(1)} %bitcast.15), channel_id=1, source_target_pairs={{0,4},{4,0},{1,5},{5,1},{2,6},{6,2},{3,7},{7,3},{8,12},{12,8},{9,1... | collective-permute-start | bytes 1572872 | tf_op jit(solution)/shard_map/ppermute | solution.py:39
  48.4 1.2 copy-start.9
  48.5 1.6 %copy-start.10 = (bf16[768,256]{1,0:T(8,128)(2,1)S(1)}, bf16[768,256]{1,0:T(8,128)(2,1)}, u32[]{:S(2)}) copy-start(bf16[768,256]{1,0:T(8,128)(2,1)} %param.13) | copy-start | bytes 1179652
  49.6 11.0 %copy-start.5 = (f32[16,256]{1,0:T(8,128)S(1)}, f32[16,256]{1,0:T(8,128)}, u32[]{:S(2)}) copy-start(f32[16,256]{1,0:T(8,128)} %branch_weight.3) | copy-start | bytes 49156
  49.6 11.0 %copy-start.6 = (f32[16,256]{1,0:T(8,128)S(1)}, f32[16,256]{1,0:T(8,128)}, u32[]{:S(2)}) copy-start(f32[16,256]{1,0:T(8,128)} %gate_weight.3) | copy-start | bytes 49156
  49.7 51.8 %copy-start.1 = (f32[128,256]{1,0:T(8,128)S(1)}, f32[128,256]{1,0:T(8,128)}, u32[]{:S(2)}) copy-start(f32[128,256]{1,0:T(8,128)} %branch_first.3) | copy-start | bytes 393220
  49.7 51.8 %copy-start.2 = (f32[128,256]{1,0:T(8,128)S(1)}, f32[128,256]{1,0:T(8,128)}, u32[]{:S(2)}) copy-start(f32[128,256]{1,0:T(8,128)} %gate_first.3) | copy-start | bytes 393220
  49.7 51.8 %copy-start.3 = (f32[128,256]{1,0:T(8,128)S(1)}, f32[128,256]{1,0:T(8,128)}, u32[]{:S(2)}) copy-start(f32[128,256]{1,0:T(8,128)} %branch_second.3) | copy-start | bytes 393220
  49.7 51.8 %copy-start.4 = (f32[128,256]{1,0:T(8,128)S(1)}, f32[128,256]{1,0:T(8,128)}, u32[]{:S(2)}) copy-start(f32[128,256]{1,0:T(8,128)} %gate_second.3) | copy-start | bytes 393220
  101.5 29.3 %copy-start.7 = (bf16[16,128]{1,0:T(8,128)(2,1)S(1)}, bf16[16,128]{1,0:T(8,128)(2,1)}, u32[]{:S(2)}) copy-start(bf16[16,128]{1,0:T(8,128)(2,1)} %gate_factor.1) | copy-start | bytes 12292
  101.5 29.3 %copy-start.8 = (bf16[16,128]{1,0:T(8,128)(2,1)S(1)}, bf16[16,128]{1,0:T(8,128)(2,1)}, u32[]{:S(2)}) copy-start(bf16[16,128]{1,0:T(8,128)(2,1)} %branch_factor.1) | copy-start | bytes 12292
  125.6 7.5 %collective-permute-start.1 = (bf16[4,2,8,16,512]{4,3,2,1,0:T(8,128)(2,1)S(1)}, bf16[4,2,8,16,512]{4,3,2,1,0:T(8,128)(2,1)S(1)}, u32[]{:S(2)}, u32[]{:S(2)}) collective-permute-start(bf16[4,2,8,16,512]{4,3,2,1,0:T(8,128)(2,1)S(1)} %all_to_all.35.mine), channel_id=1, source_target_pairs={{0,4},{4,0},{1,5},{5,1},{2,6},{6,2},{3,7},{7,3},{8,12},{12,8},{9,1... | collective-permute-start | bytes 3145736 | tf_op jit(solution)/shard_map/ppermute | solution.py:39

commit v2 on v0

--- a/solution.py
+++ b/solution.py
@@ -149,12 +149,14 @@
         new_out[...] = weight[...] + step
 
 
-def outgoing_kernel(pieces, branch_weight, gate_weight, outgoing_block):
+def outgoing_kernel(pieces, branch_weight, gate_weight, blocks):
     height = pieces.shape[1]
     block = branch_weight.shape[0]
-    outgoing_block[:height] = jnp.sum(pieces[...], axis=0)
-    outgoing_block[height : height + block] = branch_weight[...]
-    outgoing_block[height + block :] = gate_weight[...]
+    piece = jnp.sum(pieces[...], axis=0)
+    for peer in range(blocks.shape[0]):
+        blocks[peer, :height] = piece
+        blocks[peer, height : height + block] = branch_weight[...]
+        blocks[peer, height + block :] = gate_weight[...]
 
 
 def factors_kernel(mine, other, factors):
@@ -210,11 +212,11 @@
     return pltpu.CompilerParams(vmem_limit_bytes=mib << 20)
 
 
-def outgoing(pieces, branch_weight, gate_weight):
+def outgoing(pieces, branch_weight, gate_weight, peers):
     height = pieces.shape[1] + 2 * branch_weight.shape[0]
     return pl.pallas_call(
         outgoing_kernel,
-        out_shape=jax.ShapeDtypeStruct((height, pieces.shape[2]), jnp.float32),
+        out_shape=jax.ShapeDtypeStruct((peers, height, pieces.shape[2]), jnp.float32),
         in_specs=[whole()] * 3,
         out_specs=whole(),
         compiler_params=grant(4),
@@ -340,8 +342,10 @@
     )
     pieces = both.reshape(size_of(NEAR_CORES), -1, width)
     height = pieces.shape[1]
-    outgoing_block = outgoing(exchanged(pieces, NEAR_CORES), branch_weight, gate_weight)
-    arrived = lax.all_gather(outgoing_block, "zh")
+    blocks = outgoing(
+        exchanged(pieces, NEAR_CORES), branch_weight, gate_weight, size_of(FAR)
+    )
+    arrived = exchanged(blocks, FAR)
     total = arrived[:, :height].sum(axis=0)
     projected = from_everyone(total, NEAR_CORES).reshape(both.shape)
 

time: 134 us -> 134 us (level)
    all_to_all x6 -> x7, blocking collectives: 89.8 us -> 113 us  [exchanged(): return lax.all_to_all(blocks, axes, split_axis=0, concat_axis=0, tiled=True)]
    all_gather x1 -> x0, blocking collectives: 22.8 us -> none  [body(): arrived = lax.all_gather(outgoing_block, 'zh')]
where the time goes in v2:
time: 134 us
  blocking collectives  113 us (84%)
  starting transfers between devices  11.6 us (9%)
  Pallas kernels  3.76 us (3%)
  waiting for transfers between devices  1.72 us (1%)
  matrix products  1.62 us (1%)
    all_to_all x7, blocking collectives, exchanged(): return lax.all_to_all(blocks, axes, split_axis=0, concat_axis=0, tiled=True)  113 us
    ppermute x2, starting transfers between devices, swapped(): return lax.ppermute(x, 'c', [(0, 1), (1, 0)])  11.6 us
  transfers between devices with their start and end apart: 2, of which 2 were waited for; matrix products, arithmetic and copies ran while one was open for 0% of the time, Pallas kernels for 2%

profile of v2, /device:TPU:1, one launch (start us, length us, event | category | flops | bytes accessed | tf_op | source)
XLA Modules:
  0.0 133.9 jit_solution(17447375124524175114)
XLA Ops:
  0.6 0.0 copy-start
  0.7 0.9 pad_maximum_fusion.1
  1.5 27.8 %all_to_all.35.factors = bf16[8,16,256]{2,1,0:T(8,128)(2,1)S(1)} all-to-all(bf16[8,16,256]{2,1,0:T(8,128)(2,1)S(1)} %broadcast_in_dim.15), channel_id=1, replica_groups=mesh['zh'=8,'zl'=2,'x'=4,'c'=2,'tp'=4] {'zh'}, dimensions={0} | all-to-all | bytes 131072 | tf_op jit(solution)/shard_map/all_to_all | solution.py:30
  29.3 11.4 %all_to_all.36 = bf16[8,8,16,256]{3,2,1,0:T(8,128)(2,1)S(1)} all-to-all(bf16[8,8,16,256]{3,2,1,0:T(8,128)(2,1)S(1)} %broadcast_in_dim.16), channel_id=1, replica_groups=mesh['zh'=8,'zl'=2,'x'=4,'c'=2,'tp'=4] {'zl','x'}, dimensions={0} | all-to-all | bytes 1048576 | tf_op jit(solution)/shard_map/all_to_all | solution.py:30
  40.7 6.0 %collective-permute-start = (bf16[2,4,8,16,256]{4,3,2,1,0:T(8,128)(2,1)S(1)}, bf16[2,4,8,16,256]{4,3,2,1,0:T(8,128)(2,1)S(1)}, u32[]{:S(2)}, u32[]{:S(2)}) collective-permute-start(bf16[2,4,8,16,256]{4,3,2,1,0:T(8,128)(2,1)S(1)} %bitcast.20), channel_id=1, source_target_pairs={{0,4},{4,0},{1,5},{5,1},{2,6},{6,2},{3,7},{7,3},{8,12},{12,8},{9,1... | collective-permute-start | bytes 1572872 | tf_op jit(solution)/shard_map/ppermute | solution.py:38
  46.8 1.5 %collective-permute-done.other = bf16[2,4,8,16,256]{4,3,2,1,0:T(8,128)(2,1)S(1)} collective-permute-done((bf16[2,4,8,16,256]{4,3,2,1,0:T(8,128)(2,1)S(1)}, bf16[2,4,8,16,256]{4,3,2,1,0:T(8,128)(2,1)S(1)}, u32[]{:S(2)}, u32[]{:S(2)}) %collective-permute-start) | collective-permute-done | bytes 524320 | tf_op jit(solution)/shard_map/ppermute | solution.py:38
  48.3 0.1 whole_factors.1
  48.5 1.1 convolution_bitcast_fusion
  49.6 0.1 reduce-precision_convert_fusion.1
  49.7 0.3 fusion.2
  50.0 0.3 fusion.6
  50.4 10.2 %all_to_all.37.pieces = f32[16,16,256]{2,1,0:T(8,128)S(1)} all-to-all(f32[16,16,256]{2,1,0:T(8,128)S(1)} %bitcast.24), channel_id=1, replica_groups=mesh['zh'=8,'zl'=2,'x'=4,'c'=2,'tp'=4] {'zl','x','c'}, dimensions={0} | all-to-all | bytes 524288 | tf_op jit(solution)/shard_map/all_to_all | solution.py:30
  60.6 25.4 %all_to_all.38.arrived = f32[8,48,256]{2,1,0:T(8,128)S(1)} all-to-all(f32[8,48,256]{2,1,0:T(8,128)S(1)} %outgoing.1), channel_id=1, replica_groups=mesh['zh'=8,'zl'=2,'x'=4,'c'=2,'tp'=4] {'zh'}, dimensions={0} | all-to-all | bytes 786432 | tf_op jit(solution)/shard_map/all_to_all | solution.py:30
  86.0 14.6 %all_to_all.39 = f32[16,16,256]{2,1,0:T(8,128)S(1)} all-to-all(f32[16,16,256]{2,1,0:T(8,128)S(1)} %broadcast_in_dim.17), channel_id=1, replica_groups=mesh['zh'=8,'zl'=2,'x'=4,'c'=2,'tp'=4] {'zl','x','c'}, dimensions={0} | all-to-all | bytes 524288 | tf_op jit(solution)/shard_map/all_to_all | solution.py:30
  100.6 0.2 directions.1
  100.9 8.2 %all_to_all.40.squares = f32[4,8,128]{2,1,0:T(8,128)S(1)} all-to-all(f32[4,8,128]{2,1,0:T(8,128)S(1)} %broadcast_in_dim.18), channel_id=1, replica_groups=mesh['zh'=8,'zl'=2,'x'=4,'c'=2,'tp'=4] {'tp'}, dimensions={0} | all-to-all | bytes 32768 | tf_op jit(solution)/shard_map/all_to_all | solution.py:30
  109.1 0.3 new_rows.1
  109.3 0.1 broadcast_in_dim.19
  109.4 15.5 %all_to_all.41 = bf16[8,8,16,512]{3,2,1,0:T(8,128)(2,1)S(1)} all-to-all(bf16[8,8,16,512]{3,2,1,0:T(8,128)(2,1)S(1)} %broadcast_in_dim.19), channel_id=1, replica_groups=mesh['zh'=8,'zl'=2,'x'=4,'c'=2,'tp'=4] {'zl','x'}, dimensions={0} | all-to-all | bytes 2097152 | tf_op jit(solution)/shard_map/all_to_all | solution.py:30
  125.0 5.6 %collective-permute-start.1 = (bf16[2,4,8,16,512]{4,3,2,1,0:T(8,128)(2,1)S(1)}, bf16[2,4,8,16,512]{4,3,2,1,0:T(8,128)(2,1)S(1)}, u32[]{:S(2)}, u32[]{:S(2)}) collective-permute-start(bf16[2,4,8,16,512]{4,3,2,1,0:T(8,128)(2,1)S(1)} %bitcast.16), channel_id=1, source_target_pairs={{0,4},{4,0},{1,5},{5,1},{2,6},{6,2},{3,7},{7,3},{8,12},{12,8},{9,1... | collective-permute-start | bytes 3145736 | tf_op jit(solution)/shard_map/ppermute | solution.py:38
  130.6 0.9 results.1
  131.6 1.1 place_mine.1
  132.7 0.2 collective-permute-done.1.other
  132.9 1.1 place_other.1
  (29 shorter events, 0.2 us)
Async XLA Ops:
  0.6 47.8 %copy-start = (bf16[768,2048]{1,0:T(8,128)(2,1)S(1)}, bf16[768,2048]{1,0:T(8,128)(2,1)}, u32[]{:S(2)}) copy-start(bf16[768,2048]{1,0:T(8,128)(2,1)} %param.11) | copy-start | bytes 9437188
  40.7 7.6 %collective-permute-start = (bf16[2,4,8,16,256]{4,3,2,1,0:T(8,128)(2,1)S(1)}, bf16[2,4,8,16,256]{4,3,2,1,0:T(8,128)(2,1)S(1)}, u32[]{:S(2)}, u32[]{:S(2)}) collective-permute-start(bf16[2,4,8,16,256]{4,3,2,1,0:T(8,128)(2,1)S(1)} %bitcast.20), channel_id=1, source_target_pairs={{0,4},{4,0},{1,5},{5,1},{2,6},{6,2},{3,7},{7,3},{8,12},{12,8},{9,1... | collective-permute-start | bytes 1572872 | tf_op jit(solution)/shard_map/ppermute | solution.py:38
  48.4 1.2 copy-start.9
  48.4 1.6 %copy-start.10 = (bf16[768,256]{1,0:T(8,128)(2,1)S(1)}, bf16[768,256]{1,0:T(8,128)(2,1)}, u32[]{:S(2)}) copy-start(bf16[768,256]{1,0:T(8,128)(2,1)} %param.13) | copy-start | bytes 1179652
  49.6 11.0 %copy-start.5 = (f32[16,256]{1,0:T(8,128)S(1)}, f32[16,256]{1,0:T(8,128)}, u32[]{:S(2)}) copy-start(f32[16,256]{1,0:T(8,128)} %branch_weight.3) | copy-start | bytes 49156
  49.6 11.0 %copy-start.6 = (f32[16,256]{1,0:T(8,128)S(1)}, f32[16,256]{1,0:T(8,128)}, u32[]{:S(2)}) copy-start(f32[16,256]{1,0:T(8,128)} %gate_weight.3) | copy-start | bytes 49156
  49.7 50.9 %copy-start.1 = (f32[128,256]{1,0:T(8,128)S(1)}, f32[128,256]{1,0:T(8,128)}, u32[]{:S(2)}) copy-start(f32[128,256]{1,0:T(8,128)} %branch_first.3) | copy-start | bytes 393220
  49.7 50.9 %copy-start.2 = (f32[128,256]{1,0:T(8,128)S(1)}, f32[128,256]{1,0:T(8,128)}, u32[]{:S(2)}) copy-start(f32[128,256]{1,0:T(8,128)} %gate_first.3) | copy-start | bytes 393220
  49.7 50.9 %copy-start.3 = (f32[128,256]{1,0:T(8,128)S(1)}, f32[128,256]{1,0:T(8,128)}, u32[]{:S(2)}) copy-start(f32[128,256]{1,0:T(8,128)} %branch_second.3) | copy-start | bytes 393220
  49.7 50.9 %copy-start.4 = (f32[128,256]{1,0:T(8,128)S(1)}, f32[128,256]{1,0:T(8,128)}, u32[]{:S(2)}) copy-start(f32[128,256]{1,0:T(8,128)} %gate_second.3) | copy-start | bytes 393220
  85.9 44.7 %copy-start.7 = (bf16[16,128]{1,0:T(8,128)(2,1)S(1)}, bf16[16,128]{1,0:T(8,128)(2,1)}, u32[]{:S(2)}) copy-start(bf16[16,128]{1,0:T(8,128)(2,1)} %gate_factor.1) | copy-start | bytes 12292
  85.9 44.7 %copy-start.8 = (bf16[16,128]{1,0:T(8,128)(2,1)S(1)}, bf16[16,128]{1,0:T(8,128)(2,1)}, u32[]{:S(2)}) copy-start(bf16[16,128]{1,0:T(8,128)(2,1)} %branch_factor.1) | copy-start | bytes 12292
  125.0 7.9 %collective-permute-start.1 = (bf16[2,4,8,16,512]{4,3,2,1,0:T(8,128)(2,1)S(1)}, bf16[2,4,8,16,512]{4,3,2,1,0:T(8,128)(2,1)S(1)}, u32[]{:S(2)}, u32[]{:S(2)}) collective-permute-start(bf16[2,4,8,16,512]{4,3,2,1,0:T(8,128)(2,1)S(1)} %bitcast.16), channel_id=1, source_target_pairs={{0,4},{4,0},{1,5},{5,1},{2,6},{6,2},{3,7},{7,3},{8,12},{12,8},{9,1... | collective-permute-start | bytes 3145736 | tf_op jit(solution)/shard_map/ppermute | solution.py:38

commit v3 on v2

--- a/solution.py
+++ b/solution.py
@@ -9,10 +9,10 @@
 from jax.sharding import PartitionSpec as P
 
 
-FS = ("zh", "zl", "x", "c")
-FAR = ("zh",)
+FS = ("zh", "zm", "zl", "x", "c")
+FAR = ("zh", "zm")
 NEAR = ("zl", "x")
-NEAR_CORES = ("zl", "x", "c")
+NEAR_CORES = ("zm", "zl", "x", "c")
 
 first_decay = 0.8
 second_decay = 0.9
@@ -34,8 +34,8 @@
     return exchanged(jnp.broadcast_to(x, (size_of(axes), *x.shape)), axes)
 
 
-def swapped(x):
-    return lax.ppermute(x, "c", [(0, 1), (1, 0)])
+def swapped(x, axis="c"):
+    return lax.ppermute(x, axis, [(0, 1), (1, 0)])
 
 
 def two_parts(x):
@@ -96,16 +96,23 @@
     return out[:, :width] + (out[:, width : 2 * width] + out[:, 2 * width :])
 
 
-def rows_kernel(entries, squares, parts, factors, arrived, rows_new):
-    far, block, _ = factors.shape
+def rows_kernel(entries, squares, parts, factors, arrived, other, rows_new):
+    _, block, _ = factors.shape
     rank = parts.shape[1]
-    width = arrived.shape[2]
+    far, _, width = arrived.shape
+    height = arrived.shape[1] - 2 * block
+    me = lax.axis_index("zm")
     minus_scale = scale_of(entries, squares[...])
-    for p in range(2):
-        factor = factors[:, :, p * rank : (p + 1) * rank].reshape(far * block, rank)
-        step = (minus_scale * times_parts(factor, parts[p])).reshape(far, block, width)
-        weights = arrived[:, (p + 1) * block : (p + 2) * block, :]
-        rows_new[:, :, p * width : (p + 1) * width] = (weights + step).astype(jnp.bfloat16)
+    for source, place in ((arrived, me), (other, 1 - me)):
+        for p in range(2):
+            columns = slice(p * width, (p + 1) * width)
+            ranks = slice(p * rank, (p + 1) * rank)
+            factor = jnp.concatenate([factors[2 * f + place, :, ranks] for f in range(far)], axis=0)
+            step = minus_scale * times_parts(factor, parts[p])
+            for f in range(far):
+                weights = source[f, height + p * block : height + (p + 1) * block, :]
+                new = weights + step[f * block : (f + 1) * block]
+                rows_new[2 * f + place, :, columns] = new.astype(jnp.bfloat16)
 
 
 def results_kernel(
@@ -285,16 +292,16 @@
     )(projected, branch_first, gate_first, branch_second, gate_second)
 
 
-def new_rows(entries, squares, parts, factors, arrived):
+def new_rows(entries, squares, parts, factors, arrived, other):
     far, block, _ = factors.shape
     return pl.pallas_call(
         functools.partial(rows_kernel, entries),
         out_shape=jax.ShapeDtypeStruct((far, block, 2 * arrived.shape[2]), jnp.bfloat16),
-        in_specs=[whole()] * 4,
+        in_specs=[whole()] * 5,
         out_specs=whole(),
         compiler_params=grant(6),
         name="new_rows",
-    )(squares, parts, factors, arrived)
+    )(squares, parts, factors, arrived, other)
 
 
 def results(entries, projected, moments, squares, parts, factors, weights):
@@ -343,17 +350,18 @@
     pieces = both.reshape(size_of(NEAR_CORES), -1, width)
     height = pieces.shape[1]
     blocks = outgoing(
-        exchanged(pieces, NEAR_CORES), branch_weight, gate_weight, size_of(FAR)
-    )
-    arrived = exchanged(blocks, FAR)
+        exchanged(pieces, NEAR_CORES), branch_weight, gate_weight, lax.axis_size("zh")
+    )
+    arrived = exchanged(blocks, ("zh",))
     total = arrived[:, :height].sum(axis=0)
     projected = from_everyone(total, NEAR_CORES).reshape(both.shape)
+    other_arrived = swapped(arrived, "zm")
 
     entries = 2 * rank * width * lax.axis_size("tp")
     moments = (branch_first, gate_first, branch_second, gate_second)
     parts, squares = directions(projected, *moments)
     squares = from_everyone(squares, ("tp",))
-    rows_new = new_rows(entries, squares, parts, far_factors, arrived)
+    rows_new = new_rows(entries, squares, parts, far_factors, arrived, other_arrived)
 
     mine = from_everyone(rows_new, NEAR).reshape(*near, *rows_new.shape)
     other = swapped(mine)
@@ -393,7 +401,8 @@
 
 def solution(mesh):
     finer = Mesh(
-        mesh.devices.reshape(8, 2, 4, 2, mesh.shape["tp"]), ("zh", "zl", "x", "c", "tp")
+        mesh.devices.reshape(4, 2, 2, 4, 2, mesh.shape["tp"]),
+        ("zh", "zm", "zl", "x", "c", "tp"),
     )
     sharded = P(FS, None)
     split = P(FS, "tp")

time: 134 us -> 148 us (1.10)
  blocking collectives: 113 us -> 84.8 us
  starting transfers between devices: 11.6 us -> 28.8 us
  waiting for transfers between devices: 1.72 us -> 16.6 us
  local copies, waits for them, and re-layouts: 0.25 us -> 8.49 us
    all_to_all x7 -> x5, blocking collectives: 113 us -> 84.8 us  [exchanged(): return lax.all_to_all(blocks, axes, split_axis=0, concat_axis=0, tiled=True)]
    all_to_all x0 -> x2, waiting for transfers between devices: none -> 14.9 us  [exchanged(): return lax.all_to_all(blocks, axes, split_axis=0, concat_axis=0, tiled=True)]
    all_to_all x0 -> x2, starting transfers between devices: none -> 13.1 us  [exchanged(): return lax.all_to_all(blocks, axes, split_axis=0, concat_axis=0, tiled=True)]
    unnamed x22 -> x40, local copies, waits for them, and re-layouts: 0.07 us -> 7 us
    ppermute x2 -> x3, starting transfers between devices: 11.6 us -> 15.7 us  [swapped(): return lax.ppermute(x, axis, [(0, 1), (1, 0)])]
  transfers between devices with their start and end apart: 2 -> 5, of which waited for: 2 -> 4; matrix products, arithmetic and copies ran while one was open for 0% -> 0% of each run, Pallas kernels for 2% -> 2%
where the time goes in v3:
time: 148 us; the launch traced here: 147 us
  blocking collectives  84.8 us (57%)
  starting transfers between devices  28.8 us (19%)
  waiting for transfers between devices  16.6 us (11%)
  local copies, waits for them, and re-layouts  8.49 us (6%)
  Pallas kernels  4.76 us (3%)
  matrix products  1.62 us (1%)
    all_to_all x5, blocking collectives, exchanged(): return lax.all_to_all(blocks, axes, split_axis=0, concat_axis=0, tiled=True)  84.8 us
    ppermute x3, starting transfers between devices, swapped(): return lax.ppermute(x, axis, [(0, 1), (1, 0)])  15.7 us
    all_to_all x2, waiting for transfers between devices, exchanged(): return lax.all_to_all(blocks, axes, split_axis=0, concat_axis=0, tiled=True)  14.9 us
    all_to_all x2, starting transfers between devices, exchanged(): return lax.all_to_all(blocks, axes, split_axis=0, concat_axis=0, tiled=True)  13.1 us
    unnamed x40, local copies, waits for them, and re-layouts  7 us
  transfers between devices with their start and end apart: 5, of which 4 were waited for; matrix products, arithmetic and copies ran while one was open for 0% of the time, Pallas kernels for 2%

profile of v3, /device:TPU:1, one launch (start us, length us, event | category | flops | bytes accessed | tf_op | source)
XLA Modules:
  0.0 147.0 jit_solution(14056459757521871115)
XLA Ops:
  1.5 27.8 %all_to_all.35.factors = bf16[8,16,256]{2,1,0:T(8,128)(2,1)S(1)} all-to-all(bf16[8,16,256]{2,1,0:T(8,128)(2,1)S(1)} %broadcast_in_dim.15), channel_id=1, replica_groups=mesh['zh'=4,'zm'=2,'zl'=2,'x'=4,'c'=2,'tp'=4] {'zh','zm'}, dimensions={0} | all-to-all | bytes 131072 | tf_op jit(solution)/shard_map/all_to_all | solution.py:30
  29.3 11.4 %all_to_all.36 = bf16[8,8,16,256]{3,2,1,0:T(8,128)(2,1)S(1)} all-to-all(bf16[8,8,16,256]{3,2,1,0:T(8,128)(2,1)S(1)} %broadcast_in_dim.16), channel_id=1, replica_groups=mesh['zh'=4,'zm'=2,'zl'=2,'x'=4,'c'=2,'tp'=4] {'zl','x'}, dimensions={0} | all-to-all | bytes 1048576 | tf_op jit(solution)/shard_map/all_to_all | solution.py:30
  40.7 6.0 %collective-permute-start = (bf16[2,4,8,16,256]{4,3,2,1,0:T(8,128)(2,1)S(1)}, bf16[2,4,8,16,256]{4,3,2,1,0:T(8,128)(2,1)S(1)}, u32[]{:S(2)}, u32[]{:S(2)}) collective-permute-start(bf16[2,4,8,16,256]{4,3,2,1,0:T(8,128)(2,1)S(1)} %bitcast.20), channel_id=1, source_target_pairs={{0,4},{4,0},{1,5},{5,1},{2,6},{6,2},{3,7},{7,3},{8,12},{12,8},{9,1... | collective-permute-start | bytes 1572872 | tf_op jit(solution)/shard_map/ppermute | solution.py:38
  46.8 1.5 %collective-permute-done.other = bf16[2,4,8,16,256]{4,3,2,1,0:T(8,128)(2,1)S(1)} collective-permute-done((bf16[2,4,8,16,256]{4,3,2,1,0:T(8,128)(2,1)S(1)}, bf16[2,4,8,16,256]{4,3,2,1,0:T(8,128)(2,1)S(1)}, u32[]{:S(2)}, u32[]{:S(2)}) %collective-permute-start) | collective-permute-done | bytes 524320 | tf_op jit(solution)/shard_map/ppermute | solution.py:38
  48.5 1.1 convolution_bitcast_fusion
  50.3 14.2 %all_to_all.37.pieces = f32[32,8,256]{2,1,0:T(8,128)S(1)} all-to-all(f32[32,8,256]{2,1,0:T(8,128)S(1)} %bitcast.24), channel_id=1, replica_groups=mesh['zh'=4,'zm'=2,'zl'=2,'x'=4,'c'=2,'tp'=4] {'zm','zl','x','c'}, dimensions={0} | all-to-all | bytes 524288 | tf_op jit(solution)/shard_map/all_to_all | solution.py:30
  64.6 16.1 %all_to_all.38.arrived = f32[4,40,256]{2,1,0:T(8,128)S(1)} all-to-all(f32[4,40,256]{2,1,0:T(8,128)S(1)} %outgoing.1), channel_id=1, replica_groups=mesh['zh'=4,'zm'=2,'zl'=2,'x'=4,'c'=2,'tp'=4] {'zh'}, dimensions={0} | all-to-all | bytes 327680 | tf_op jit(solution)/shard_map/all_to_all | solution.py:30
  82.0 8.9 %all-to-all-start.4 = ((f32[32,8,256]{2,1,0:T(8,128)}), f32[32,8,256]{2,1,0:T(8,128)S(1)}, u32[]{:S(2)}, u32[]{:S(2)}) async-start(f32[32,8,256]{2,1,0:T(8,128)} %broadcast_in_dim.17), calls=%async_computation.4 | async-start | bytes 524288 | tf_op jit(solution)/shard_map/all_to_all | solution.py:30
  90.9 4.2 %collective-permute-start.1 = (f32[4,40,256]{2,1,0:T(8,128)}, f32[4,40,256]{2,1,0:T(8,128)}, u32[]{:S(2)}, u32[]{:S(2)}) collective-permute-start(f32[4,40,256]{2,1,0:T(8,128)} %copy-done.4), channel_id=1, source_target_pairs={{0,64},{64,0},{1,65},{65,1},{2,66},{66,2},{3,67},{67,3},{4,68},{68... | collective-permute-start | bytes 491528 | tf_op jit(solution)/shard_map/ppermute | solution.py:38
  95.1 10.7 %all-to-all-done.4 = f32[32,8,256]{2,1,0:T(8,128)S(1)} async-done(((f32[32,8,256]{2,1,0:T(8,128)}), f32[32,8,256]{2,1,0:T(8,128)S(1)}, u32[]{:S(2)}, u32[]{:S(2)}) %all-to-all-start.4) | async-done | bytes 262176 | tf_op jit(solution)/shard_map/all_to_all | solution.py:30
  105.8 0.9 copy-done.6
  106.7 0.9 copy-done.8
  107.6 0.9 copy-done.10
  108.5 0.9 copy-done.12
  111.0 4.2 %all-to-all-start.5 = ((f32[4,8,128]{2,1,0:T(8,128)}), f32[4,8,128]{2,1,0:T(8,128)S(1)}, u32[]{:S(2)}, u32[]{:S(2)}) async-start(f32[4,8,128]{2,1,0:T(8,128)} %broadcast_in_dim.18), calls=%async_computation.5 | async-start | bytes 32768 | tf_op jit(solution)/shard_map/all_to_all | solution.py:30
  115.2 4.2 %all-to-all-done.5.squares = f32[4,8,128]{2,1,0:T(8,128)S(1)} async-done(((f32[4,8,128]{2,1,0:T(8,128)}), f32[4,8,128]{2,1,0:T(8,128)S(1)}, u32[]{:S(2)}, u32[]{:S(2)}) %all-to-all-start.5) | async-done | bytes 16416 | tf_op jit(solution)/shard_map/all_to_all | solution.py:30
  119.4 1.0 copy-done.2
  120.4 0.9 copy-done.5
  121.3 1.3 new_rows.1
  122.7 15.4 %all_to_all.39 = bf16[8,8,16,512]{3,2,1,0:T(8,128)(2,1)S(1)} all-to-all(bf16[8,8,16,512]{3,2,1,0:T(8,128)(2,1)S(1)} %broadcast_in_dim.19), channel_id=1, replica_groups=mesh['zh'=4,'zm'=2,'zl'=2,'x'=4,'c'=2,'tp'=4] {'zl','x'}, dimensions={0} | all-to-all | bytes 2097152 | tf_op jit(solution)/shard_map/all_to_all | solution.py:30
  138.1 5.5 %collective-permute-start.2 = (bf16[2,4,8,16,512]{4,3,2,1,0:T(8,128)(2,1)S(1)}, bf16[2,4,8,16,512]{4,3,2,1,0:T(8,128)(2,1)S(1)}, u32[]{:S(2)}, u32[]{:S(2)}) collective-permute-start(bf16[2,4,8,16,512]{4,3,2,1,0:T(8,128)(2,1)S(1)} %bitcast.16), channel_id=1, source_target_pairs={{0,4},{4,0},{1,5},{5,1},{2,6},{6,2},{3,7},{7,3},{8,12},{12,8},{9,1... | collective-permute-start | bytes 3145736 | tf_op jit(solution)/shard_map/ppermute | solution.py:38
  143.7 0.9 results.1
  144.7 1.1 place_mine.1
  145.9 1.1 place_other.1
  (51 shorter events, 5.1 us)
Async XLA Ops:
  0.6 47.8 %copy-start = (bf16[768,2048]{1,0:T(8,128)(2,1)S(1)}, bf16[768,2048]{1,0:T(8,128)(2,1)}, u32[]{:S(2)}) copy-start(bf16[768,2048]{1,0:T(8,128)(2,1)} %param.11) | copy-start | bytes 9437188
  40.7 7.6 %collective-permute-start = (bf16[2,4,8,16,256]{4,3,2,1,0:T(8,128)(2,1)S(1)}, bf16[2,4,8,16,256]{4,3,2,1,0:T(8,128)(2,1)S(1)}, u32[]{:S(2)}, u32[]{:S(2)}) collective-permute-start(bf16[2,4,8,16,256]{4,3,2,1,0:T(8,128)(2,1)S(1)} %bitcast.20), channel_id=1, source_target_pairs={{0,4},{4,0},{1,5},{5,1},{2,6},{6,2},{3,7},{7,3},{8,12},{12,8},{9,1... | collective-permute-start | bytes 1572872 | tf_op jit(solution)/shard_map/ppermute | solution.py:38
  48.4 1.2 copy-start.18
  48.4 1.5 %copy-start.19 = (bf16[768,256]{1,0:T(8,128)(2,1)S(1)}, bf16[768,256]{1,0:T(8,128)(2,1)}, u32[]{:S(2)}) copy-start(bf16[768,256]{1,0:T(8,128)(2,1)} %param.13) | copy-start | bytes 1179652
  49.6 15.0 %copy-start.14 = (f32[16,256]{1,0:T(8,128)S(1)}, f32[16,256]{1,0:T(8,128)}, u32[]{:S(2)}) copy-start(f32[16,256]{1,0:T(8,128)} %branch_weight.3) | copy-start | bytes 49156
  49.6 15.0 %copy-start.15 = (f32[16,256]{1,0:T(8,128)S(1)}, f32[16,256]{1,0:T(8,128)}, u32[]{:S(2)}) copy-start(f32[16,256]{1,0:T(8,128)} %gate_weight.3) | copy-start | bytes 49156
  64.6 79.1 %copy-start.16 = (bf16[16,128]{1,0:T(8,128)(2,1)S(1)}, bf16[16,128]{1,0:T(8,128)(2,1)}, u32[]{:S(2)}) copy-start(bf16[16,128]{1,0:T(8,128)(2,1)} %gate_factor.1) | copy-start | bytes 12292
  64.6 79.1 %copy-start.17 = (bf16[16,128]{1,0:T(8,128)(2,1)S(1)}, bf16[16,128]{1,0:T(8,128)(2,1)}, u32[]{:S(2)}) copy-start(bf16[16,128]{1,0:T(8,128)(2,1)} %branch_factor.1) | copy-start | bytes 12292
  82.0 23.8 %all-to-all-start.4 = ((f32[32,8,256]{2,1,0:T(8,128)}), f32[32,8,256]{2,1,0:T(8,128)S(1)}, u32[]{:S(2)}, u32[]{:S(2)}) async-start(f32[32,8,256]{2,1,0:T(8,128)} %broadcast_in_dim.17), calls=%async_computation.4 | async-start | bytes 524288 | tf_op jit(solution)/shard_map/all_to_all | solution.py:30
  90.9 24.3 %collective-permute-start.1 = (f32[4,40,256]{2,1,0:T(8,128)}, f32[4,40,256]{2,1,0:T(8,128)}, u32[]{:S(2)}, u32[]{:S(2)}) collective-permute-start(f32[4,40,256]{2,1,0:T(8,128)} %copy-done.4), channel_id=1, source_target_pairs={{0,64},{64,0},{1,65},{65,1},{2,66},{66,2},{3,67},{67,3},{4,68},{68... | collective-permute-start | bytes 491528 | tf_op jit(solution)/shard_map/ppermute | solution.py:38
  105.8 0.9 copy-start.6
  106.7 0.9 copy-start.8
  107.6 0.9 copy-start.10
  108.5 0.9 copy-start.12
  109.7 0.7 copy-start.1
  111.0 8.4 %all-to-all-start.5 = ((f32[4,8,128]{2,1,0:T(8,128)}), f32[4,8,128]{2,1,0:T(8,128)S(1)}, u32[]{:S(2)}, u32[]{:S(2)}) async-start(f32[4,8,128]{2,1,0:T(8,128)} %broadcast_in_dim.18), calls=%async_computation.5 | async-start | bytes 32768 | tf_op jit(solution)/shard_map/all_to_all | solution.py:30
  119.4 1.0 copy-start.2
  120.4 0.9 copy-start.5
  121.3 22.4 %copy-start.3 = (bf16[2,128,768]{2,1,0:T(8,128)(2,1)S(1)}, bf16[2,128,768]{2,1,0:T(8,128)(2,1)}, u32[]{:S(2)}) copy-start(bf16[2,128,768]{2,1,0:T(8,128)(2,1)} %copy-done.1) | copy-start | bytes 1179652
  121.3 22.4 %copy-start.7 = (f32[128,256]{1,0:T(8,128)S(1)}, f32[128,256]{1,0:T(8,128)}, u32[]{:S(2)}) copy-start(f32[128,256]{1,0:T(8,128)} %branch_first.3) | copy-start | bytes 393220
  121.3 22.4 %copy-start.9 = (f32[128,256]{1,0:T(8,128)S(1)}, f32[128,256]{1,0:T(8,128)}, u32[]{:S(2)}) copy-start(f32[128,256]{1,0:T(8,128)} %gate_first.3) | copy-start | bytes 393220
  121.3 22.4 %copy-start.11 = (f32[128,256]{1,0:T(8,128)S(1)}, f32[128,256]{1,0:T(8,128)}, u32[]{:S(2)}) copy-start(f32[128,256]{1,0:T(8,128)} %branch_second.3) | copy-start | bytes 393220
  121.3 22.4 %copy-start.13 = (f32[128,256]{1,0:T(8,128)S(1)}, f32[128,256]{1,0:T(8,128)}, u32[]{:S(2)}) copy-start(f32[128,256]{1,0:T(8,128)} %gate_second.3) | copy-start | bytes 393220
  138.1 7.8 %collective-permute-start.2 = (bf16[2,4,8,16,512]{4,3,2,1,0:T(8,128)(2,1)S(1)}, bf16[2,4,8,16,512]{4,3,2,1,0:T(8,128)(2,1)S(1)}, u32[]{:S(2)}, u32[]{:S(2)}) collective-permute-start(bf16[2,4,8,16,512]{4,3,2,1,0:T(8,128)(2,1)S(1)} %bitcast.16), channel_id=1, source_target_pairs={{0,4},{4,0},{1,5},{5,1},{2,6},{6,2},{3,7},{7,3},{8,12},{12,8},{9,1... | collective-permute-start | bytes 3145736 | tf_op jit(solution)/shard_map/ppermute | solution.py:38
  (1 other events, 0.7 us)

commit v4 on v3

--- a/solution.py
+++ b/solution.py
@@ -12,7 +12,7 @@
 FS = ("zh", "zm", "zl", "x", "c")
 FAR = ("zh", "zm")
 NEAR = ("zl", "x")
-NEAR_CORES = ("zm", "zl", "x", "c")
+NEAR_CORES = ("zl", "x", "c")
 
 first_decay = 0.8
 second_decay = 0.9
@@ -96,21 +96,20 @@
     return out[:, :width] + (out[:, width : 2 * width] + out[:, 2 * width :])
 
 
-def rows_kernel(entries, squares, parts, factors, arrived, other, rows_new):
+def rows_kernel(entries, squares, parts, factors, mine, other, rows_new):
     _, block, _ = factors.shape
     rank = parts.shape[1]
-    far, _, width = arrived.shape
-    height = arrived.shape[1] - 2 * block
+    far, _, width = mine.shape
     me = lax.axis_index("zm")
     minus_scale = scale_of(entries, squares[...])
-    for source, place in ((arrived, me), (other, 1 - me)):
+    for source, place in ((mine, me), (other, 1 - me)):
         for p in range(2):
             columns = slice(p * width, (p + 1) * width)
             ranks = slice(p * rank, (p + 1) * rank)
             factor = jnp.concatenate([factors[2 * f + place, :, ranks] for f in range(far)], axis=0)
             step = minus_scale * times_parts(factor, parts[p])
             for f in range(far):
-                weights = source[f, height + p * block : height + (p + 1) * block, :]
+                weights = source[f, p * block : (p + 1) * block, :]
                 new = weights + step[f * block : (f + 1) * block]
                 rows_new[2 * f + place, :, columns] = new.astype(jnp.bfloat16)
 
@@ -292,16 +291,16 @@
     )(projected, branch_first, gate_first, branch_second, gate_second)
 
 
-def new_rows(entries, squares, parts, factors, arrived, other):
+def new_rows(entries, squares, parts, factors, mine, other):
     far, block, _ = factors.shape
     return pl.pallas_call(
         functools.partial(rows_kernel, entries),
-        out_shape=jax.ShapeDtypeStruct((far, block, 2 * arrived.shape[2]), jnp.bfloat16),
+        out_shape=jax.ShapeDtypeStruct((far, block, 2 * mine.shape[2]), jnp.bfloat16),
         in_specs=[whole()] * 5,
         out_specs=whole(),
         compiler_params=grant(6),
         name="new_rows",
-    )(squares, parts, factors, arrived, other)
+    )(squares, parts, factors, mine, other)
 
 
 def results(entries, projected, moments, squares, parts, factors, weights):
@@ -353,15 +352,17 @@
         exchanged(pieces, NEAR_CORES), branch_weight, gate_weight, lax.axis_size("zh")
     )
     arrived = exchanged(blocks, ("zh",))
-    total = arrived[:, :height].sum(axis=0)
-    projected = from_everyone(total, NEAR_CORES).reshape(both.shape)
-    other_arrived = swapped(arrived, "zm")
+    partial = arrived[:, :height].sum(axis=0)
+    weights = arrived[:, height:]
+    other_partial = swapped(partial, "zm")
+    other_weights = swapped(weights, "zm")
+    projected = from_everyone(partial + other_partial, NEAR_CORES).reshape(both.shape)
 
     entries = 2 * rank * width * lax.axis_size("tp")
     moments = (branch_first, gate_first, branch_second, gate_second)
     parts, squares = directions(projected, *moments)
     squares = from_everyone(squares, ("tp",))
-    rows_new = new_rows(entries, squares, parts, far_factors, arrived, other_arrived)
+    rows_new = new_rows(entries, squares, parts, far_factors, weights, other_weights)
 
     mine = from_everyone(rows_new, NEAR).reshape(*near, *rows_new.shape)
     other = swapped(mine)

time: 148 us -> 143 us (0.966)
  waiting for transfers between devices: 16.6 us -> 9.46 us
  starting transfers between devices: 28.8 us -> 34.6 us
  blocking collectives: 84.8 us -> 80.3 us
    all_to_all x2, waiting for transfers between devices: 14.9 us -> 6.67 us  [exchanged(): return lax.all_to_all(blocks, axes, split_axis=0, concat_axis=0, tiled=True)]
    ppermute x3 -> x4, starting transfers between devices: 15.7 us -> 23.5 us  [swapped(): return lax.ppermute(x, axis, [(0, 1), (1, 0)])]
    all_to_all x5, blocking collectives: 84.8 us -> 80.3 us  [exchanged(): return lax.all_to_all(blocks, axes, split_axis=0, concat_axis=0, tiled=True)]
    all_to_all x2, starting transfers between devices: 13.1 us -> 11.2 us  [exchanged(): return lax.all_to_all(blocks, axes, split_axis=0, concat_axis=0, tiled=True)]
    slice x0 -> x1, local copies, waits for them, and re-layouts: none -> 1.57 us  [body(): weights = arrived[:, height:]]
    unnamed x40 -> x38, local copies, waits for them, and re-layouts: 7 us -> 6.09 us
  transfers between devices with their start and end apart: 5 -> 6, of which waited for: 4 -> 5; matrix products, arithmetic and copies ran while one was open for 0% -> 2% of each run, Pallas kernels for 2% -> 2%
where the time goes in v4:
time: 143 us; the launch traced here: 142 us
  blocking collectives  80.3 us (56%)
  starting transfers between devices  34.6 us (24%)
  waiting for transfers between devices  9.46 us (7%)
  local copies, waits for them, and re-layouts  9.16 us (6%)
  Pallas kernels  4.8 us (3%)
  matrix products  1.62 us (1%)
    all_to_all x5, blocking collectives, exchanged(): return lax.all_to_all(blocks, axes, split_axis=0, concat_axis=0, tiled=True)  80.3 us
    ppermute x4, starting transfers between devices, swapped(): return lax.ppermute(x, axis, [(0, 1), (1, 0)])  23.5 us
    all_to_all x2, starting transfers between devices, exchanged(): return lax.all_to_all(blocks, axes, split_axis=0, concat_axis=0, tiled=True)  11.2 us
    all_to_all x2, waiting for transfers between devices, exchanged(): return lax.all_to_all(blocks, axes, split_axis=0, concat_axis=0, tiled=True)  6.67 us
    unnamed x38, local copies, waits for them, and re-layouts  6.09 us
  transfers between devices with their start and end apart: 6, of which 5 were waited for; matrix products, arithmetic and copies ran while one was open for 2% of the time, Pallas kernels for 2%

profile of v4, /device:TPU:1, one launch (start us, length us, event | category | flops | bytes accessed | tf_op | source)
XLA Modules:
  0.0 142.0 jit_solution(1508246928185142172)
XLA Ops:
  1.5 27.8 %all_to_all.35.factors = bf16[8,16,256]{2,1,0:T(8,128)(2,1)S(1)} all-to-all(bf16[8,16,256]{2,1,0:T(8,128)(2,1)S(1)} %broadcast_in_dim.15), channel_id=1, replica_groups=mesh['zh'=4,'zm'=2,'zl'=2,'x'=4,'c'=2,'tp'=4] {'zh','zm'}, dimensions={0} | all-to-all | bytes 131072 | tf_op jit(solution)/shard_map/all_to_all | solution.py:30
  29.3 11.4 %all_to_all.36 = bf16[8,8,16,256]{3,2,1,0:T(8,128)(2,1)S(1)} all-to-all(bf16[8,8,16,256]{3,2,1,0:T(8,128)(2,1)S(1)} %broadcast_in_dim.16), channel_id=1, replica_groups=mesh['zh'=4,'zm'=2,'zl'=2,'x'=4,'c'=2,'tp'=4] {'zl','x'}, dimensions={0} | all-to-all | bytes 1048576 | tf_op jit(solution)/shard_map/all_to_all | solution.py:30
  40.7 6.0 %collective-permute-start = (bf16[2,4,8,16,256]{4,3,2,1,0:T(8,128)(2,1)S(1)}, bf16[2,4,8,16,256]{4,3,2,1,0:T(8,128)(2,1)S(1)}, u32[]{:S(2)}, u32[]{:S(2)}) collective-permute-start(bf16[2,4,8,16,256]{4,3,2,1,0:T(8,128)(2,1)S(1)} %bitcast.20), channel_id=1, source_target_pairs={{0,4},{4,0},{1,5},{5,1},{2,6},{6,2},{3,7},{7,3},{8,12},{12,8},{9,1... | collective-permute-start | bytes 1572872 | tf_op jit(solution)/shard_map/ppermute | solution.py:38
  46.8 1.5 %collective-permute-done.other = bf16[2,4,8,16,256]{4,3,2,1,0:T(8,128)(2,1)S(1)} collective-permute-done((bf16[2,4,8,16,256]{4,3,2,1,0:T(8,128)(2,1)S(1)}, bf16[2,4,8,16,256]{4,3,2,1,0:T(8,128)(2,1)S(1)}, u32[]{:S(2)}, u32[]{:S(2)}) %collective-permute-start) | collective-permute-done | bytes 524320 | tf_op jit(solution)/shard_map/ppermute | solution.py:38
  48.5 1.1 convolution_bitcast_fusion
  50.3 10.2 %all_to_all.37.pieces = f32[16,16,256]{2,1,0:T(8,128)S(1)} all-to-all(f32[16,16,256]{2,1,0:T(8,128)S(1)} %bitcast.24), channel_id=1, replica_groups=mesh['zh'=4,'zm'=2,'zl'=2,'x'=4,'c'=2,'tp'=4] {'zl','x','c'}, dimensions={0} | all-to-all | bytes 524288 | tf_op jit(solution)/shard_map/all_to_all | solution.py:30
  60.5 15.6 %all_to_all.38 = f32[4,48,256]{2,1,0:T(8,128)S(1)} all-to-all(f32[4,48,256]{2,1,0:T(8,128)S(1)} %outgoing.1), channel_id=1, replica_groups=mesh['zh'=4,'zm'=2,'zl'=2,'x'=4,'c'=2,'tp'=4] {'zh'}, dimensions={0} | all-to-all | bytes 393216 | tf_op jit(solution)/shard_map/all_to_all | solution.py:30
  76.8 8.6 %collective-permute-start.1 = (f32[16,256]{1,0:T(8,128)S(1)}, f32[16,256]{1,0:T(8,128)S(1)}, u32[]{:S(2)}, u32[]{:S(2)}) collective-permute-start(f32[16,256]{1,0:T(8,128)S(1)} %slice_reduce_fusion), channel_id=1, source_target_pairs={{0,64},{64,0},{1,65},{65,1},{2,66},{66,2},{3,67},{67,3},{4,68},{68... | collective-permute-start | bytes 49160 | tf_op jit(solution)/shard_map/ppermute | solution.py:38
  85.4 1.1 collective-permute-done.1
  87.2 7.0 %all-to-all-start.4 = ((f32[16,16,256]{2,1,0:T(8,128)}), f32[16,16,256]{2,1,0:T(8,128)S(1)}, u32[]{:S(2)}, u32[]{:S(2)}) async-start(f32[16,16,256]{2,1,0:T(8,128)} %broadcast_in_dim.17), calls=%async_computation.4 | async-start | bytes 524288 | tf_op jit(solution)/shard_map/all_to_all | solution.py:30
  94.2 1.6 %slice.39.mine = f32[4,32,256]{2,1,0:T(8,128)} slice(f32[4,48,256]{2,1,0:T(8,128)} %copy-done.16), slice={[0:4], [16:48], [0:256]} | slice | bytes 262144 | tf_op jit(solution)/shard_map/slice | solution.py:356
  95.8 3.2 %collective-permute-start.2 = (f32[4,32,256]{2,1,0:T(8,128)}, f32[4,32,256]{2,1,0:T(8,128)}, u32[]{:S(2)}, u32[]{:S(2)}) collective-permute-start(f32[4,32,256]{2,1,0:T(8,128)} %slice.39.mine), channel_id=1, source_target_pairs={{0,64},{64,0},{1,65},{65,1},{2,66},{66,2},{3,67},{67,3},{4,68},{68... | collective-permute-start | bytes 393224 | tf_op jit(solution)/shard_map/ppermute | solution.py:38
  98.9 2.5 %all-to-all-done.4 = f32[16,16,256]{2,1,0:T(8,128)S(1)} async-done(((f32[16,16,256]{2,1,0:T(8,128)}), f32[16,16,256]{2,1,0:T(8,128)S(1)}, u32[]{:S(2)}, u32[]{:S(2)}) %all-to-all-start.4) | async-done | bytes 262176 | tf_op jit(solution)/shard_map/all_to_all | solution.py:30
  101.4 0.9 copy-done.4
  102.3 0.9 copy-done.6
  106.6 4.2 %all-to-all-start.5 = ((f32[4,8,128]{2,1,0:T(8,128)}), f32[4,8,128]{2,1,0:T(8,128)S(1)}, u32[]{:S(2)}, u32[]{:S(2)}) async-start(f32[4,8,128]{2,1,0:T(8,128)} %broadcast_in_dim.18), calls=%async_computation.5 | async-start | bytes 32768 | tf_op jit(solution)/shard_map/all_to_all | solution.py:30
  110.8 4.2 %all-to-all-done.5.squares = f32[4,8,128]{2,1,0:T(8,128)S(1)} async-done(((f32[4,8,128]{2,1,0:T(8,128)}), f32[4,8,128]{2,1,0:T(8,128)S(1)}, u32[]{:S(2)}, u32[]{:S(2)}) %all-to-all-start.5) | async-done | bytes 16416 | tf_op jit(solution)/shard_map/all_to_all | solution.py:30
  115.0 1.0 copy-done.2
  116.0 1.3 new_rows.1
  117.4 15.5 %all_to_all.39 = bf16[8,8,16,512]{3,2,1,0:T(8,128)(2,1)S(1)} all-to-all(bf16[8,8,16,512]{3,2,1,0:T(8,128)(2,1)S(1)} %broadcast_in_dim.19), channel_id=1, replica_groups=mesh['zh'=4,'zm'=2,'zl'=2,'x'=4,'c'=2,'tp'=4] {'zl','x'}, dimensions={0} | all-to-all | bytes 2097152 | tf_op jit(solution)/shard_map/all_to_all | solution.py:30
  132.9 5.7 %collective-permute-start.3 = (bf16[2,4,8,16,512]{4,3,2,1,0:T(8,128)(2,1)S(1)}, bf16[2,4,8,16,512]{4,3,2,1,0:T(8,128)(2,1)S(1)}, u32[]{:S(2)}, u32[]{:S(2)}) collective-permute-start(bf16[2,4,8,16,512]{4,3,2,1,0:T(8,128)(2,1)S(1)} %bitcast.16), channel_id=1, source_target_pairs={{0,4},{4,0},{1,5},{5,1},{2,6},{6,2},{3,7},{7,3},{8,12},{12,8},{9,1... | collective-permute-start | bytes 3145736 | tf_op jit(solution)/shard_map/ppermute | solution.py:38
  138.7 0.9 results.1
  139.6 1.1 place_mine.1
  140.9 1.1 place_other.1
  (53 shorter events, 6.9 us)
Async XLA Ops:
  0.6 47.8 %copy-start = (bf16[768,2048]{1,0:T(8,128)(2,1)S(1)}, bf16[768,2048]{1,0:T(8,128)(2,1)}, u32[]{:S(2)}) copy-start(bf16[768,2048]{1,0:T(8,128)(2,1)} %param.11) | copy-start | bytes 9437188
  40.7 7.6 %collective-permute-start = (bf16[2,4,8,16,256]{4,3,2,1,0:T(8,128)(2,1)S(1)}, bf16[2,4,8,16,256]{4,3,2,1,0:T(8,128)(2,1)S(1)}, u32[]{:S(2)}, u32[]{:S(2)}) collective-permute-start(bf16[2,4,8,16,256]{4,3,2,1,0:T(8,128)(2,1)S(1)} %bitcast.20), channel_id=1, source_target_pairs={{0,4},{4,0},{1,5},{5,1},{2,6},{6,2},{3,7},{7,3},{8,12},{12,8},{9,1... | collective-permute-start | bytes 1572872 | tf_op jit(solution)/shard_map/ppermute | solution.py:38
  48.4 1.2 copy-start.17
  48.4 1.5 %copy-start.18 = (bf16[768,256]{1,0:T(8,128)(2,1)S(1)}, bf16[768,256]{1,0:T(8,128)(2,1)}, u32[]{:S(2)}) copy-start(bf16[768,256]{1,0:T(8,128)(2,1)} %param.13) | copy-start | bytes 1179652
  49.6 10.9 %copy-start.12 = (f32[16,256]{1,0:T(8,128)S(1)}, f32[16,256]{1,0:T(8,128)}, u32[]{:S(2)}) copy-start(f32[16,256]{1,0:T(8,128)} %branch_weight.3) | copy-start | bytes 49156
  49.6 10.9 %copy-start.13 = (f32[16,256]{1,0:T(8,128)S(1)}, f32[16,256]{1,0:T(8,128)}, u32[]{:S(2)}) copy-start(f32[16,256]{1,0:T(8,128)} %gate_weight.3) | copy-start | bytes 49156
  76.8 61.8 %copy-start.14 = (bf16[16,128]{1,0:T(8,128)(2,1)S(1)}, bf16[16,128]{1,0:T(8,128)(2,1)}, u32[]{:S(2)}) copy-start(bf16[16,128]{1,0:T(8,128)(2,1)} %gate_factor.1) | copy-start | bytes 12292
  76.8 61.9 %copy-start.15 = (bf16[16,128]{1,0:T(8,128)(2,1)S(1)}, bf16[16,128]{1,0:T(8,128)(2,1)}, u32[]{:S(2)}) copy-start(bf16[16,128]{1,0:T(8,128)(2,1)} %branch_factor.1) | copy-start | bytes 12292
  76.8 9.7 %collective-permute-start.1 = (f32[16,256]{1,0:T(8,128)S(1)}, f32[16,256]{1,0:T(8,128)S(1)}, u32[]{:S(2)}, u32[]{:S(2)}) collective-permute-start(f32[16,256]{1,0:T(8,128)S(1)} %slice_reduce_fusion), channel_id=1, source_target_pairs={{0,64},{64,0},{1,65},{65,1},{2,66},{66,2},{3,67},{67,3},{4,68},{68... | collective-permute-start | bytes 49160 | tf_op jit(solution)/shard_map/ppermute | solution.py:38
  87.2 14.2 %all-to-all-start.4 = ((f32[16,16,256]{2,1,0:T(8,128)}), f32[16,16,256]{2,1,0:T(8,128)S(1)}, u32[]{:S(2)}, u32[]{:S(2)}) async-start(f32[16,16,256]{2,1,0:T(8,128)} %broadcast_in_dim.17), calls=%async_computation.4 | async-start | bytes 524288 | tf_op jit(solution)/shard_map/all_to_all | solution.py:30
  95.8 15.0 %collective-permute-start.2 = (f32[4,32,256]{2,1,0:T(8,128)}, f32[4,32,256]{2,1,0:T(8,128)}, u32[]{:S(2)}, u32[]{:S(2)}) collective-permute-start(f32[4,32,256]{2,1,0:T(8,128)} %slice.39.mine), channel_id=1, source_target_pairs={{0,64},{64,0},{1,65},{65,1},{2,66},{66,2},{3,67},{67,3},{4,68},{68... | collective-permute-start | bytes 393224 | tf_op jit(solution)/shard_map/ppermute | solution.py:38
  101.4 0.9 copy-start.4
  102.3 0.9 copy-start.6
  103.2 0.9 copy-start.8
  104.1 0.9 copy-start.10
  105.2 0.7 copy-start.1
  106.6 8.4 %all-to-all-start.5 = ((f32[4,8,128]{2,1,0:T(8,128)}), f32[4,8,128]{2,1,0:T(8,128)S(1)}, u32[]{:S(2)}, u32[]{:S(2)}) async-start(f32[4,8,128]{2,1,0:T(8,128)} %broadcast_in_dim.18), calls=%async_computation.5 | async-start | bytes 32768 | tf_op jit(solution)/shard_map/all_to_all | solution.py:30
  115.0 1.0 copy-start.2
  116.0 22.6 %copy-start.3 = (bf16[2,128,768]{2,1,0:T(8,128)(2,1)S(1)}, bf16[2,128,768]{2,1,0:T(8,128)(2,1)}, u32[]{:S(2)}) copy-start(bf16[2,128,768]{2,1,0:T(8,128)(2,1)} %copy-done.1) | copy-start | bytes 1179652
  116.0 22.6 %copy-start.5 = (f32[128,256]{1,0:T(8,128)S(1)}, f32[128,256]{1,0:T(8,128)}, u32[]{:S(2)}) copy-start(f32[128,256]{1,0:T(8,128)} %branch_first.3) | copy-start | bytes 393220
  116.0 22.6 %copy-start.7 = (f32[128,256]{1,0:T(8,128)S(1)}, f32[128,256]{1,0:T(8,128)}, u32[]{:S(2)}) copy-start(f32[128,256]{1,0:T(8,128)} %gate_first.3) | copy-start | bytes 393220
  116.0 22.7 %copy-start.9 = (f32[128,256]{1,0:T(8,128)S(1)}, f32[128,256]{1,0:T(8,128)}, u32[]{:S(2)}) copy-start(f32[128,256]{1,0:T(8,128)} %branch_second.3) | copy-start | bytes 393220
  116.0 22.7 %copy-start.11 = (f32[128,256]{1,0:T(8,128)S(1)}, f32[128,256]{1,0:T(8,128)}, u32[]{:S(2)}) copy-start(f32[128,256]{1,0:T(8,128)} %gate_second.3) | copy-start | bytes 393220
  132.9 7.9 %collective-permute-start.3 = (bf16[2,4,8,16,512]{4,3,2,1,0:T(8,128)(2,1)S(1)}, bf16[2,4,8,16,512]{4,3,2,1,0:T(8,128)(2,1)S(1)}, u32[]{:S(2)}, u32[]{:S(2)}) collective-permute-start(bf16[2,4,8,16,512]{4,3,2,1,0:T(8,128)(2,1)S(1)} %bitcast.16), channel_id=1, source_target_pairs={{0,4},{4,0},{1,5},{5,1},{2,6},{6,2},{3,7},{7,3},{8,12},{12,8},{9,1... | collective-permute-start | bytes 3145736 | tf_op jit(solution)/shard_map/ppermute | solution.py:38
  (1 other events, 0.7 us)

commit v5 on v4

--- a/solution.py
+++ b/solution.py
@@ -111,7 +111,8 @@
             for f in range(far):
                 weights = source[f, p * block : (p + 1) * block, :]
                 new = weights + step[f * block : (f + 1) * block]
-                rows_new[2 * f + place, :, columns] = new.astype(jnp.bfloat16)
+                for peer in range(rows_new.shape[0]):
+                    rows_new[peer, 2 * f + place, :, columns] = new.astype(jnp.bfloat16)
 
 
 def results_kernel(
@@ -165,6 +166,23 @@
         blocks[peer, height + block :] = gate_weight[...]
 
 
+def total_kernel(mine, other, blocks):
+    total = mine[...] + other[...]
+    for peer in range(blocks.shape[0]):
+        blocks[peer] = total
+
+
+def totals(mine, other, peers):
+    return pl.pallas_call(
+        total_kernel,
+        out_shape=jax.ShapeDtypeStruct((peers, *mine.shape), mine.dtype),
+        in_specs=[whole()] * 2,
+        out_specs=whole(),
+        compiler_params=grant(2),
+        name="totals",
+    )(mine, other)
+
+
 def factors_kernel(mine, other, factors):
     near_z, near_x, far, block, _ = mine.shape
     core = lax.axis_index("c")
@@ -291,11 +309,11 @@
     )(projected, branch_first, gate_first, branch_second, gate_second)
 
 
-def new_rows(entries, squares, parts, factors, mine, other):
+def new_rows(entries, squares, parts, factors, mine, other, peers):
     far, block, _ = factors.shape
     return pl.pallas_call(
         functools.partial(rows_kernel, entries),
-        out_shape=jax.ShapeDtypeStruct((far, block, 2 * mine.shape[2]), jnp.bfloat16),
+        out_shape=jax.ShapeDtypeStruct((peers, far, block, 2 * mine.shape[2]), jnp.bfloat16),
         in_specs=[whole()] * 5,
         out_specs=whole(),
         compiler_params=grant(6),
@@ -356,15 +374,18 @@
     weights = arrived[:, height:]
     other_partial = swapped(partial, "zm")
     other_weights = swapped(weights, "zm")
-    projected = from_everyone(partial + other_partial, NEAR_CORES).reshape(both.shape)
+    sums = totals(partial, other_partial, size_of(NEAR_CORES))
+    projected = exchanged(sums, NEAR_CORES).reshape(both.shape)
 
     entries = 2 * rank * width * lax.axis_size("tp")
     moments = (branch_first, gate_first, branch_second, gate_second)
     parts, squares = directions(projected, *moments)
     squares = from_everyone(squares, ("tp",))
-    rows_new = new_rows(entries, squares, parts, far_factors, weights, other_weights)
-
-    mine = from_everyone(rows_new, NEAR).reshape(*near, *rows_new.shape)
+    rows_new = new_rows(
+        entries, squares, parts, far_factors, weights, other_weights, size_of(NEAR)
+    )
+
+    mine = exchanged(rows_new, NEAR).reshape(*near, *rows_new.shape[1:])
     other = swapped(mine)
     copies = place_mine(mine)
     (

time: 143 us -> 142 us (level)
    unnamed x38 -> x40, local copies, waits for them, and re-layouts: 6.09 us -> 6.12 us
where the time goes in v5:
time: 142 us; the launch traced here: 141 us
  blocking collectives  80.3 us (57%)
  starting transfers between devices  34.5 us (24%)
  waiting for transfers between devices  9.46 us (7%)
  local copies, waits for them, and re-layouts  8.34 us (6%)
  Pallas kernels  4.84 us (3%)
  matrix products  1.62 us (1%)
    all_to_all x5, blocking collectives, exchanged(): return lax.all_to_all(blocks, axes, split_axis=0, concat_axis=0, tiled=True)  80.3 us
    ppermute x4, starting transfers between devices, swapped(): return lax.ppermute(x, axis, [(0, 1), (1, 0)])  23.3 us
    all_to_all x2, starting transfers between devices, exchanged(): return lax.all_to_all(blocks, axes, split_axis=0, concat_axis=0, tiled=True)  11.2 us
    all_to_all x2, waiting for transfers between devices, exchanged(): return lax.all_to_all(blocks, axes, split_axis=0, concat_axis=0, tiled=True)  6.67 us
    unnamed x40, local copies, waits for them, and re-layouts  6.12 us
  transfers between devices with their start and end apart: 6, of which 5 were waited for; matrix products, arithmetic and copies ran while one was open for 2% of the time, Pallas kernels for 2%

profile of v5, /device:TPU:1, one launch (start us, length us, event | category | flops | bytes accessed | tf_op | source)
XLA Modules:
  0.0 141.1 jit_solution(4053206775249725410)
XLA Ops:
  1.5 27.8 %all_to_all.35.factors = bf16[8,16,256]{2,1,0:T(8,128)(2,1)S(1)} all-to-all(bf16[8,16,256]{2,1,0:T(8,128)(2,1)S(1)} %broadcast_in_dim.9), channel_id=1, replica_groups=mesh['zh'=4,'zm'=2,'zl'=2,'x'=4,'c'=2,'tp'=4] {'zh','zm'}, dimensions={0} | all-to-all | bytes 131072 | tf_op jit(solution)/shard_map/all_to_all | solution.py:30
  29.3 11.4 %all_to_all.36 = bf16[8,8,16,256]{3,2,1,0:T(8,128)(2,1)S(1)} all-to-all(bf16[8,8,16,256]{3,2,1,0:T(8,128)(2,1)S(1)} %broadcast_in_dim.10), channel_id=1, replica_groups=mesh['zh'=4,'zm'=2,'zl'=2,'x'=4,'c'=2,'tp'=4] {'zl','x'}, dimensions={0} | all-to-all | bytes 1048576 | tf_op jit(solution)/shard_map/all_to_all | solution.py:30
  40.7 6.0 %collective-permute-start = (bf16[2,4,8,16,256]{4,3,2,1,0:T(8,128)(2,1)S(1)}, bf16[2,4,8,16,256]{4,3,2,1,0:T(8,128)(2,1)S(1)}, u32[]{:S(2)}, u32[]{:S(2)}) collective-permute-start(bf16[2,4,8,16,256]{4,3,2,1,0:T(8,128)(2,1)S(1)} %bitcast.20), channel_id=1, source_target_pairs={{0,4},{4,0},{1,5},{5,1},{2,6},{6,2},{3,7},{7,3},{8,12},{12,8},{9,1... | collective-permute-start | bytes 1572872 | tf_op jit(solution)/shard_map/ppermute | solution.py:38
  46.8 1.5 %collective-permute-done.other = bf16[2,4,8,16,256]{4,3,2,1,0:T(8,128)(2,1)S(1)} collective-permute-done((bf16[2,4,8,16,256]{4,3,2,1,0:T(8,128)(2,1)S(1)}, bf16[2,4,8,16,256]{4,3,2,1,0:T(8,128)(2,1)S(1)}, u32[]{:S(2)}, u32[]{:S(2)}) %collective-permute-start) | collective-permute-done | bytes 524320 | tf_op jit(solution)/shard_map/ppermute | solution.py:38
  48.5 1.1 convolution_bitcast_fusion
  50.3 10.2 %all_to_all.37.pieces = f32[16,16,256]{2,1,0:T(8,128)S(1)} all-to-all(f32[16,16,256]{2,1,0:T(8,128)S(1)} %bitcast.24), channel_id=1, replica_groups=mesh['zh'=4,'zm'=2,'zl'=2,'x'=4,'c'=2,'tp'=4] {'zl','x','c'}, dimensions={0} | all-to-all | bytes 524288 | tf_op jit(solution)/shard_map/all_to_all | solution.py:30
  60.5 15.6 %all_to_all.38 = f32[4,48,256]{2,1,0:T(8,128)S(1)} all-to-all(f32[4,48,256]{2,1,0:T(8,128)S(1)} %outgoing.1), channel_id=1, replica_groups=mesh['zh'=4,'zm'=2,'zl'=2,'x'=4,'c'=2,'tp'=4] {'zh'}, dimensions={0} | all-to-all | bytes 393216 | tf_op jit(solution)/shard_map/all_to_all | solution.py:30
  76.1 8.5 %collective-permute-start.1 = (f32[16,256]{1,0:T(8,128)S(1)}, f32[16,256]{1,0:T(8,128)S(1)}, u32[]{:S(2)}, u32[]{:S(2)}) collective-permute-start(f32[16,256]{1,0:T(8,128)S(1)} %slice_reduce_fusion.mine), channel_id=1, source_target_pairs={{0,64},{64,0},{1,65},{65,1},{2,66},{66,2},{3,67},{67,3},{4,68},{68... | collective-permute-start | bytes 49160 | tf_op jit(solution)/shard_map/ppermute | solution.py:38
  84.6 1.1 collective-permute-done.1.other
  86.4 7.0 %all-to-all-start.4 = ((f32[16,16,256]{2,1,0:T(8,128)}), f32[16,16,256]{2,1,0:T(8,128)S(1)}, u32[]{:S(2)}, u32[]{:S(2)}) async-start(f32[16,16,256]{2,1,0:T(8,128)} %copy-done.4), calls=%async_computation.4 | async-start | bytes 524288 | tf_op jit(solution)/shard_map/all_to_all | solution.py:30
  93.4 1.6 %slice.39.mine = f32[4,32,256]{2,1,0:T(8,128)} slice(f32[4,48,256]{2,1,0:T(8,128)} %copy-done.17), slice={[0:4], [16:48], [0:256]} | slice | bytes 262144 | tf_op jit(solution)/shard_map/slice | solution.py:374
  95.0 3.2 %collective-permute-start.2 = (f32[4,32,256]{2,1,0:T(8,128)}, f32[4,32,256]{2,1,0:T(8,128)}, u32[]{:S(2)}, u32[]{:S(2)}) collective-permute-start(f32[4,32,256]{2,1,0:T(8,128)} %slice.39.mine), channel_id=1, source_target_pairs={{0,64},{64,0},{1,65},{65,1},{2,66},{66,2},{3,67},{67,3},{4,68},{68... | collective-permute-start | bytes 393224 | tf_op jit(solution)/shard_map/ppermute | solution.py:38
  98.2 2.5 %all-to-all-done.4 = f32[16,16,256]{2,1,0:T(8,128)S(1)} async-done(((f32[16,16,256]{2,1,0:T(8,128)}), f32[16,16,256]{2,1,0:T(8,128)S(1)}, u32[]{:S(2)}, u32[]{:S(2)}) %all-to-all-start.4) | async-done | bytes 262176 | tf_op jit(solution)/shard_map/all_to_all | solution.py:30
  100.6 0.9 copy-done.5
  101.5 0.9 copy-done.7
  105.8 4.2 %all-to-all-start.5 = ((f32[4,8,128]{2,1,0:T(8,128)}), f32[4,8,128]{2,1,0:T(8,128)S(1)}, u32[]{:S(2)}, u32[]{:S(2)}) async-start(f32[4,8,128]{2,1,0:T(8,128)} %broadcast_in_dim.11), calls=%async_computation.5 | async-start | bytes 32768 | tf_op jit(solution)/shard_map/all_to_all | solution.py:30
  110.0 4.2 %all-to-all-done.5.squares = f32[4,8,128]{2,1,0:T(8,128)S(1)} async-done(((f32[4,8,128]{2,1,0:T(8,128)}), f32[4,8,128]{2,1,0:T(8,128)S(1)}, u32[]{:S(2)}, u32[]{:S(2)}) %all-to-all-start.5) | async-done | bytes 16416 | tf_op jit(solution)/shard_map/all_to_all | solution.py:30
  114.2 1.0 copy-done.2
  115.2 1.3 new_rows.1
  116.6 15.5 %all_to_all.39 = bf16[8,8,16,512]{3,2,1,0:T(8,128)(2,1)S(1)} all-to-all(bf16[8,8,16,512]{3,2,1,0:T(8,128)(2,1)S(1)} %new_rows.1), channel_id=1, replica_groups=mesh['zh'=4,'zm'=2,'zl'=2,'x'=4,'c'=2,'tp'=4] {'zl','x'}, dimensions={0} | all-to-all | bytes 2097152 | tf_op jit(solution)/shard_map/all_to_all | solution.py:30
  132.0 5.7 %collective-permute-start.3 = (bf16[2,4,8,16,512]{4,3,2,1,0:T(8,128)(2,1)S(1)}, bf16[2,4,8,16,512]{4,3,2,1,0:T(8,128)(2,1)S(1)}, u32[]{:S(2)}, u32[]{:S(2)}) collective-permute-start(bf16[2,4,8,16,512]{4,3,2,1,0:T(8,128)(2,1)S(1)} %bitcast.16), channel_id=1, source_target_pairs={{0,4},{4,0},{1,5},{5,1},{2,6},{6,2},{3,7},{7,3},{8,12},{12,8},{9,1... | collective-permute-start | bytes 3145736 | tf_op jit(solution)/shard_map/ppermute | solution.py:38
  137.8 0.9 results.1
  138.7 1.1 place_mine.1
  140.0 1.1 place_other.1
  (53 shorter events, 6.1 us)
Async XLA Ops:
  0.6 47.8 %copy-start = (bf16[768,2048]{1,0:T(8,128)(2,1)S(1)}, bf16[768,2048]{1,0:T(8,128)(2,1)}, u32[]{:S(2)}) copy-start(bf16[768,2048]{1,0:T(8,128)(2,1)} %param.11) | copy-start | bytes 9437188
  40.7 7.6 %collective-permute-start = (bf16[2,4,8,16,256]{4,3,2,1,0:T(8,128)(2,1)S(1)}, bf16[2,4,8,16,256]{4,3,2,1,0:T(8,128)(2,1)S(1)}, u32[]{:S(2)}, u32[]{:S(2)}) collective-permute-start(bf16[2,4,8,16,256]{4,3,2,1,0:T(8,128)(2,1)S(1)} %bitcast.20), channel_id=1, source_target_pairs={{0,4},{4,0},{1,5},{5,1},{2,6},{6,2},{3,7},{7,3},{8,12},{12,8},{9,1... | collective-permute-start | bytes 1572872 | tf_op jit(solution)/shard_map/ppermute | solution.py:38
  48.4 1.2 copy-start.18
  48.4 1.5 %copy-start.19 = (bf16[768,256]{1,0:T(8,128)(2,1)S(1)}, bf16[768,256]{1,0:T(8,128)(2,1)}, u32[]{:S(2)}) copy-start(bf16[768,256]{1,0:T(8,128)(2,1)} %param.13) | copy-start | bytes 1179652
  49.6 10.9 %copy-start.13 = (f32[16,256]{1,0:T(8,128)S(1)}, f32[16,256]{1,0:T(8,128)}, u32[]{:S(2)}) copy-start(f32[16,256]{1,0:T(8,128)} %branch_weight.3) | copy-start | bytes 49156
  49.6 10.9 %copy-start.14 = (f32[16,256]{1,0:T(8,128)S(1)}, f32[16,256]{1,0:T(8,128)}, u32[]{:S(2)}) copy-start(f32[16,256]{1,0:T(8,128)} %gate_weight.3) | copy-start | bytes 49156
  60.5 77.2 %copy-start.15 = (bf16[16,128]{1,0:T(8,128)(2,1)S(1)}, bf16[16,128]{1,0:T(8,128)(2,1)}, u32[]{:S(2)}) copy-start(bf16[16,128]{1,0:T(8,128)(2,1)} %gate_factor.1) | copy-start | bytes 12292
  60.5 77.2 %copy-start.16 = (bf16[16,128]{1,0:T(8,128)(2,1)S(1)}, bf16[16,128]{1,0:T(8,128)(2,1)}, u32[]{:S(2)}) copy-start(bf16[16,128]{1,0:T(8,128)(2,1)} %branch_factor.1) | copy-start | bytes 12292
  76.1 9.6 %copy-start.17 = (f32[4,48,256]{2,1,0:T(8,128)}, f32[4,48,256]{2,1,0:T(8,128)S(1)}, u32[]{:S(2)}) copy-start(f32[4,48,256]{2,1,0:T(8,128)S(1)} %all_to_all.38) | copy-start | bytes 589828
  76.1 9.6 %collective-permute-start.1 = (f32[16,256]{1,0:T(8,128)S(1)}, f32[16,256]{1,0:T(8,128)S(1)}, u32[]{:S(2)}, u32[]{:S(2)}) collective-permute-start(f32[16,256]{1,0:T(8,128)S(1)} %slice_reduce_fusion.mine), channel_id=1, source_target_pairs={{0,64},{64,0},{1,65},{65,1},{2,66},{66,2},{3,67},{67,3},{4,68},{68... | collective-permute-start | bytes 49160 | tf_op jit(solution)/shard_map/ppermute | solution.py:38
  86.4 14.2 %all-to-all-start.4 = ((f32[16,16,256]{2,1,0:T(8,128)}), f32[16,16,256]{2,1,0:T(8,128)S(1)}, u32[]{:S(2)}, u32[]{:S(2)}) async-start(f32[16,16,256]{2,1,0:T(8,128)} %copy-done.4), calls=%async_computation.4 | async-start | bytes 524288 | tf_op jit(solution)/shard_map/all_to_all | solution.py:30
  95.0 15.0 %collective-permute-start.2 = (f32[4,32,256]{2,1,0:T(8,128)}, f32[4,32,256]{2,1,0:T(8,128)}, u32[]{:S(2)}, u32[]{:S(2)}) collective-permute-start(f32[4,32,256]{2,1,0:T(8,128)} %slice.39.mine), channel_id=1, source_target_pairs={{0,64},{64,0},{1,65},{65,1},{2,66},{66,2},{3,67},{67,3},{4,68},{68... | collective-permute-start | bytes 393224 | tf_op jit(solution)/shard_map/ppermute | solution.py:38
  100.6 0.9 copy-start.5
  101.5 0.9 copy-start.7
  102.4 0.9 copy-start.9
  103.3 0.9 copy-start.11
  105.8 8.4 %all-to-all-start.5 = ((f32[4,8,128]{2,1,0:T(8,128)}), f32[4,8,128]{2,1,0:T(8,128)S(1)}, u32[]{:S(2)}, u32[]{:S(2)}) async-start(f32[4,8,128]{2,1,0:T(8,128)} %broadcast_in_dim.11), calls=%async_computation.5 | async-start | bytes 32768 | tf_op jit(solution)/shard_map/all_to_all | solution.py:30
  114.2 1.0 copy-start.2
  115.2 22.5 %copy-start.3 = (bf16[2,128,768]{2,1,0:T(8,128)(2,1)S(1)}, bf16[2,128,768]{2,1,0:T(8,128)(2,1)}, u32[]{:S(2)}) copy-start(bf16[2,128,768]{2,1,0:T(8,128)(2,1)} %copy-done.1) | copy-start | bytes 1179652
  115.2 22.5 %copy-start.6 = (f32[128,256]{1,0:T(8,128)S(1)}, f32[128,256]{1,0:T(8,128)}, u32[]{:S(2)}) copy-start(f32[128,256]{1,0:T(8,128)} %branch_first.3) | copy-start | bytes 393220
  115.2 22.5 %copy-start.8 = (f32[128,256]{1,0:T(8,128)S(1)}, f32[128,256]{1,0:T(8,128)}, u32[]{:S(2)}) copy-start(f32[128,256]{1,0:T(8,128)} %gate_first.3) | copy-start | bytes 393220
  115.2 22.6 %copy-start.10 = (f32[128,256]{1,0:T(8,128)S(1)}, f32[128,256]{1,0:T(8,128)}, u32[]{:S(2)}) copy-start(f32[128,256]{1,0:T(8,128)} %branch_second.3) | copy-start | bytes 393220
  115.2 22.6 %copy-start.12 = (f32[128,256]{1,0:T(8,128)S(1)}, f32[128,256]{1,0:T(8,128)}, u32[]{:S(2)}) copy-start(f32[128,256]{1,0:T(8,128)} %gate_second.3) | copy-start | bytes 393220
  132.0 8.0 %collective-permute-start.3 = (bf16[2,4,8,16,512]{4,3,2,1,0:T(8,128)(2,1)S(1)}, bf16[2,4,8,16,512]{4,3,2,1,0:T(8,128)(2,1)S(1)}, u32[]{:S(2)}, u32[]{:S(2)}) collective-permute-start(bf16[2,4,8,16,512]{4,3,2,1,0:T(8,128)(2,1)S(1)} %bitcast.16), channel_id=1, source_target_pairs={{0,4},{4,0},{1,5},{5,1},{2,6},{6,2},{3,7},{7,3},{8,12},{12,8},{9,1... | collective-permute-start | bytes 3145736 | tf_op jit(solution)/shard_map/ppermute | solution.py:38
  (2 other events, 1.5 us)
